TPU v7x, 128 devices: a whole 4x4x4 slice. The times are simulated.
128 devices in a mesh: sp: 32 (over z, y, core), tp: 4 (over x).
Axes of the slice: x: 4, y: 4, z: 4, core: 2. Of those that a mesh axis runs over, the one named last changes fastest.
Arguments:
- tokens: bfloat16 [12288, 2048], P(('sp', 'tp')), may hold values from -8 to 8, as said below
- query_weight: bfloat16 [2048, 1024], P(None, 'tp'), as said below
- key_weight: bfloat16 [2048, 256], P(None, 'tp'), as said below
- value_weight: bfloat16 [2048, 256], P(None, 'tp'), may hold values from -0.125 to 0.125
- out_weight: bfloat16 [1024, 2048], P('tp'), may hold values from -0.75 to 0.75
- query_gain: bfloat16 [16, 64], P('tp'), may hold values from 0.5 to 6.5
- key_gain: bfloat16 [4, 64], P('tp'), may hold values from 0.5 to 6.5
Outputs:
- mixed: bfloat16 [12288, 2048], P(('sp', 'tp'))
- log_sums: float32 [16, 12288], P('tp', 'sp')
Inputs may be any that keep to these rules, and one draw needn't show every extreme that they name: Each block of 384 consecutive tokens has a mean vector of its own. `query_weight`: entries are those of a weight over 2048 inputs, of magnitude at most 6 / sqrt(2048). `key_weight`: entries are those of a weight over 2048 inputs, of magnitude at most 6 / sqrt(2048).
All inputs are finite; a program needn't handle non-finite values.
Results may differ from a plain program's by a relative error of at most 0.028.
Values may be sent and summed in bfloat16 or wider, within the bound.
A program may use at most 64 MiB of HBM per device.

v0:
```python
import math

import jax
import jax.numpy as jnp
from jax import lax
from jax.sharding import PartitionSpec as P

GRID_W = 64


ROPE_BASE = 10000.0


def in_order(tiles, dim):
    dims = list(tiles.shape[1:])
    dims[dim] *= tiles.shape[0]
    return jnp.moveaxis(tiles, 0, dim).reshape(dims)


def copy_for_each(array, axis):
    count = lax.axis_size(axis)
    return lax.all_to_all(
        jnp.broadcast_to(array[None], (count, *array.shape)), axis, 0, 0, tiled=True
    )


def collect(array, axis, dim):
    return in_order(copy_for_each(array, axis), dim)


def side_by_side(arrays, axis, dim, along):
    widths = [a.shape[along] for a in arrays]
    both = jnp.concatenate(arrays, axis=along)
    out = lax.all_gather(both, axis, axis=dim, tiled=True)
    return tuple(jnp.split(out, [sum(widths[:k]) for k in range(1, len(widths))], axis=along))


def angle_tables(first, count, quarter):
    place = first + jnp.arange(count, dtype=jnp.int32)
    grid_row = (place // GRID_W).astype(jnp.float32)
    grid_col = (place % GRID_W).astype(jnp.float32)
    freq = ROPE_BASE ** (-jnp.arange(quarter, dtype=jnp.float32) / quarter)
    row_angle = grid_row[:, None] * freq[None, :]
    col_angle = grid_col[:, None] * freq[None, :]
    return (jnp.cos(row_angle), jnp.sin(row_angle), jnp.cos(col_angle), jnp.sin(col_angle))


def turn_pairs(part, cosine, sine):
    quarter = part.shape[-1] // 2
    first = part[..., :quarter]
    second = part[..., quarter:]
    cosine = cosine[:, None, :]
    sine = sine[:, None, :]
    return jnp.concatenate(
        [first * cosine - second * sine, second * cosine + first * sine], axis=-1
    )


def prepare(raw, gain, first):
    count = raw.shape[0]
    heads, width = gain.shape
    values = raw.astype(jnp.float32).reshape(count, heads, width)
    scaled = values * lax.rsqrt(jnp.mean(values * values, axis=-1, keepdims=True) + 1e-06)
    scaled = scaled * gain.astype(jnp.float32)[None, :, :]
    row_cos, row_sin, col_cos, col_sin = angle_tables(first, count, width // 4)
    half = width // 2
    turned = jnp.concatenate(
        [
            turn_pairs(scaled[..., :half], row_cos, row_sin),
            turn_pairs(scaled[..., half:], col_cos, col_sin),
        ],
        axis=-1,
    )
    return turned.astype(jnp.bfloat16)


def group_queries(queries, kv_count):
    count, heads, width = queries.shape
    share = heads // kv_count
    grouped = queries.reshape(count, kv_count, share, width).transpose(1, 0, 2, 3)
    return grouped.reshape(kv_count, count * share, width)


def start_state(kv_count, query_rows, width):
    top = jnp.full((kv_count, query_rows), -1e30, jnp.float32)
    total = jnp.zeros((kv_count, query_rows), jnp.float32)
    summed = jnp.zeros((kv_count, query_rows, width), jnp.float32)
    return (top, total, summed)


def fold_keys(state, pieces, grouped, scale):
    keys, values = pieces
    count, kv_count, width = keys.shape
    block_len = math.gcd(count, 1024)
    key_blocks = keys.reshape(count // block_len, block_len, kv_count, width)
    value_blocks = values.reshape(count // block_len, block_len, kv_count, width)

    def inner(carry, block):
        top, total, summed = carry
        key_block, value_block = block
        scores = (
            lax.dot_general(
                grouped, key_block, (((2,), (2,)), ((0,), (1,))), preferred_element_type=jnp.float32
            )
            * scale
        )
        new_top = jnp.maximum(top, jnp.max(scores, axis=-1))
        factor = jnp.exp(top - new_top)
        expo = jnp.exp(scores - new_top[..., None])
        total = total * factor + jnp.sum(expo, axis=-1)
        mixed = lax.dot_general(
            expo.astype(jnp.bfloat16),
            value_block,
            (((2,), (0,)), ((0,), (1,))),
            preferred_element_type=jnp.float32,
        )
        summed = summed * factor[..., None] + mixed
        return ((new_top, total, summed), None)

    state, _ = lax.scan(inner, state, (key_blocks, value_blocks))
    return state


def finish(state, count, share):
    top, total, summed = state
    kv_count, query_rows, width = summed.shape
    attended = (summed / total[..., None]).astype(jnp.bfloat16)
    attended = attended.reshape(kv_count, count, share, width).transpose(1, 0, 2, 3)
    attended = attended.reshape(count, kv_count * share * width)
    log_rows = (top + jnp.log(total)).reshape(kv_count, count, share).transpose(0, 2, 1)
    return (attended, log_rows.reshape(kv_count * share, count))


def body(tokens, query_weight, key_weight, value_weight, out_weight, query_gain, key_gain):
    width = query_gain.shape[1]
    scale = width ** (-0.5)
    query_cols = query_weight.shape[1]
    key_cols = key_weight.shape[1]
    kv_count = key_gain.shape[0]
    share = query_gain.shape[0] // kv_count
    piece = collect(tokens, "tp", 0)
    made = [
        jnp.dot(piece, weight, preferred_element_type=jnp.float32).astype(jnp.bfloat16)
        for weight in (query_weight, key_weight, value_weight)
    ]
    joined = jnp.concatenate(made, axis=1)
    count = joined.shape[0]
    first = lax.axis_index("sp") * count
    queries = prepare(joined[:, :query_cols], query_gain, first)
    keys = prepare(joined[:, query_cols : query_cols + key_cols], key_gain, first)
    values = joined[:, query_cols + key_cols :].reshape(count, kv_count, width)
    grouped = group_queries(queries, kv_count)
    state = fold_keys(
        start_state(kv_count, count * share, width),
        side_by_side((keys, values), "sp", 0, 1),
        grouped=grouped,
        scale=scale,
    )
    attended, log_sums = finish(state, count, share)
    mixed = lax.psum_scatter(
        jnp.dot(attended, out_weight, preferred_element_type=jnp.float32).astype(jnp.bfloat16),
        "tp",
        scatter_dimension=0,
        tiled=True,
    )
    return (mixed, log_sums)


def solution(mesh):
    return jax.shard_map(
        body,
        mesh=mesh,
        in_specs=(
            P(("sp", "tp"), None),
            P(None, "tp"),
            P(None, "tp"),
            P(None, "tp"),
            P("tp", None),
            P("tp", None),
            P("tp", None),
        ),
        out_specs=(P(("sp", "tp"), None), P("tp", "sp")),
        check_vma=False,
    )
```

profile of v0, /device:TPU:0, one launch (start us, length us, event | category | flops | bytes accessed | tf_op | source)
XLA Modules:
  0.0 175.0 jit_solution(1470406230783409071)
XLA Ops:
  7.2 2.4 %broadcast_in_dim.11 = bf16[4,96,2048]{2,1,0:T(8,128)(2,1)} broadcast(bf16[96,2048]{1,0:T(8,128)(2,1)} %param.9), dimensions={1,2} | broadcast | bytes 1966080 | tf_op jit(solution)/shard_map/broadcast_in_dim | solution.py:23
  9.6 4.5 %all-to-all-start = ((bf16[4,96,2048]{2,1,0:T(8,128)(2,1)}), bf16[4,96,2048]{2,1,0:T(8,128)(2,1)S(1)}, u32[]{:S(2)}, u32[]{:S(2)}) async-start(bf16[4,96,2048]{2,1,0:T(8,128)(2,1)} %broadcast_in_dim.11), calls=%async_computation | async-start | bytes 3145728 | tf_op jit(solution)/shard_map/all_to_all | solution.py:22
  14.2 20.7 %all-to-all-done = bf16[4,96,2048]{2,1,0:T(8,128)(2,1)S(1)} async-done(((bf16[4,96,2048]{2,1,0:T(8,128)(2,1)}), bf16[4,96,2048]{2,1,0:T(8,128)(2,1)S(1)}, u32[]{:S(2)}, u32[]{:S(2)}) %all-to-all-start) | async-done | bytes 1572896 | tf_op jit(solution)/shard_map/all_to_all | solution.py:22
  34.9 0.6 fusion.23
  35.5 0.6 multiply_reduce_fusion.1
  36.1 0.1 multiply_bitcast_fusion
  36.2 0.3 fusion.39
  36.5 0.7 pad_maximum_fusion.1
  37.2 0.3 multiply_cosine_fusion.1
  37.5 2.0 %fusion.24 = (f32[384,4]{0,1:T(4,128)S(1)}, bf16[384,256]{0,1:T(8,128)(2,1)S(1)}) fusion(bf16[384,2048]{1,0:T(8,128)(2,1)S(1)} %bitcast.62, bf16[2048,256]{1,0:T(8,128)(2,1)} %param.10), kind=kOutput, calls=%fused_computation.34 | convolution fusion | flops 403044864 | bytes 2824192 | tf_op jit(solution)/shard_map/dot_general | solution.py:143
  39.5 0.1 fusion.25
  39.6 0.1 subtract_convert_fusion.1
  39.7 0.3 copy.18
  39.9 0.3 copy.17
  40.2 0.3 copy.16
  40.5 0.3 copy.15
  40.7 0.5 pad_maximum_fusion
  41.2 43.2 %all-gather.2.cloned.1.call-done = bf16[12288,2,64]{0,2,1:T(8,128)(2,1)} async-done(((bf16[384,2,64]{0,2,1:T(8,128)(2,1)}), bf16[12288,2,64]{0,2,1:T(8,128)(2,1)}) %all-gather.2.cloned.1.call-update) | async-done | bytes 3145744 | tf_op jit(solution)/shard_map/all_gather | solution.py:34
  84.4 2.2 %fusion.47 = (bf16[12288,1,64]{0,2,1:T(8,128)(2,1)S(1)}, bf16[12288,1,64]{0,2,1:T(8,128)(2,1)S(1)}) fusion(bf16[12288,2,64]{0,2,1:T(8,128)(2,1)} %all-gather.2.cloned.1.call-done), kind=kLoop, calls=%fused_computation.86 | loop fusion | bytes 6291456 | tf_op jit(solution)/shard_map/split | solution.py:35
  86.6 0.1 copy.28
  86.7 1.3 copy.27
  88.0 52.6 %while.15 = (s32[]{:T(128)}, f32[1,1536]{1,0:T(1,128)S(1)}, f32[1,1536]{1,0:T(1,128)S(1)}, f32[1,1536,64]{1,2,0:T(8,128)S(1)}, bf16[12,1024,1,64]{1,3,2,0:T(8,12...) while((s32[]{:T(128)}, f32[1,1536]{1,0:T(1,128)S(1)}, ...), condition=%wide.region_5.6_spmd.clone, body=%wide.region_2.5_spmd.clone.sunk | while | flops 415540224 | bytes 20420728 | solution.py:120
  88.0 1.0 multiply_reduce_fusion.3
  89.1 1.1 fusion.65
  90.2 2.2 %fusion.67 = f32[1,1536,64]{1,2,0:T(8,128)S(1)} fusion(f32[1024,1536]{1,0:T(8,128)S(1)} %get-tuple-element.181, f32[1536]{0:T(1024)S(1)} %get-tuple-element.182, f32[1,1536,64]{1,2,0:T(8,128)S(1)} %get-tuple-element.196, f32[1536]{0:T(1024)S(1)} %get-tuple-element.183, pred[]{:T(512)S(6)} %compare.14, ...), kind=kOutput, calls=%fused_computation.6.clone.1 | convolution fusion | flops 206340096 | bytes 7221253 | tf_op jit(solution)/shard_map/while/body/eval_jaxpr/dot_general | solution.py:111
  92.4 1.0 multiply_reduce_fusion.3
  93.5 1.1 fusion.65
  94.6 2.2 %fusion.67 = f32[1,1536,64]{1,2,0:T(8,128)S(1)} fusion(f32[1024,1536]{1,0:T(8,128)S(1)} %get-tuple-element.181, f32[1536]{0:T(1024)S(1)} %get-tuple-element.182, f32[1,1536,64]{1,2,0:T(8,128)S(1)} %get-tuple-element.196, f32[1536]{0:T(1024)S(1)} %get-tuple-element.183, pred[]{:T(512)S(6)} %compare.14, ...), kind=kOutput, calls=%fused_computation.6.clone.1 | convolution fusion | flops 206340096 | bytes 7221253 | tf_op jit(solution)/shard_map/while/body/eval_jaxpr/dot_general | solution.py:111
  96.8 1.0 multiply_reduce_fusion.3
  97.9 1.1 fusion.65
  99.0 2.2 %fusion.67 = f32[1,1536,64]{1,2,0:T(8,128)S(1)} fusion(f32[1024,1536]{1,0:T(8,128)S(1)} %get-tuple-element.181, f32[1536]{0:T(1024)S(1)} %get-tuple-element.182, f32[1,1536,64]{1,2,0:T(8,128)S(1)} %get-tuple-element.196, f32[1536]{0:T(1024)S(1)} %get-tuple-element.183, pred[]{:T(512)S(6)} %compare.14, ...), kind=kOutput, calls=%fused_computation.6.clone.1 | convolution fusion | flops 206340096 | bytes 7221253 | tf_op jit(solution)/shard_map/while/body/eval_jaxpr/dot_general | solution.py:111
  101.2 1.0 multiply_reduce_fusion.3
  102.3 1.1 fusion.65
  103.4 2.2 %fusion.67 = f32[1,1536,64]{1,2,0:T(8,128)S(1)} fusion(f32[1024,1536]{1,0:T(8,128)S(1)} %get-tuple-element.181, f32[1536]{0:T(1024)S(1)} %get-tuple-element.182, f32[1,1536,64]{1,2,0:T(8,128)S(1)} %get-tuple-element.196, f32[1536]{0:T(1024)S(1)} %get-tuple-element.183, pred[]{:T(512)S(6)} %compare.14, ...), kind=kOutput, calls=%fused_computation.6.clone.1 | convolution fusion | flops 206340096 | bytes 7221253 | tf_op jit(solution)/shard_map/while/body/eval_jaxpr/dot_general | solution.py:111
  105.6 1.0 multiply_reduce_fusion.3
  106.7 1.1 fusion.65
  107.8 2.2 %fusion.67 = f32[1,1536,64]{1,2,0:T(8,128)S(1)} fusion(f32[1024,1536]{1,0:T(8,128)S(1)} %get-tuple-element.181, f32[1536]{0:T(1024)S(1)} %get-tuple-element.182, f32[1,1536,64]{1,2,0:T(8,128)S(1)} %get-tuple-element.196, f32[1536]{0:T(1024)S(1)} %get-tuple-element.183, pred[]{:T(512)S(6)} %compare.14, ...), kind=kOutput, calls=%fused_computation.6.clone.1 | convolution fusion | flops 206340096 | bytes 7221253 | tf_op jit(solution)/shard_map/while/body/eval_jaxpr/dot_general | solution.py:111
  110.0 1.0 multiply_reduce_fusion.3
  111.1 1.1 fusion.65
  112.2 2.2 %fusion.67 = f32[1,1536,64]{1,2,0:T(8,128)S(1)} fusion(f32[1024,1536]{1,0:T(8,128)S(1)} %get-tuple-element.181, f32[1536]{0:T(1024)S(1)} %get-tuple-element.182, f32[1,1536,64]{1,2,0:T(8,128)S(1)} %get-tuple-element.196, f32[1536]{0:T(1024)S(1)} %get-tuple-element.183, pred[]{:T(512)S(6)} %compare.14, ...), kind=kOutput, calls=%fused_computation.6.clone.1 | convolution fusion | flops 206340096 | bytes 7221253 | tf_op jit(solution)/shard_map/while/body/eval_jaxpr/dot_general | solution.py:111
  114.4 1.0 multiply_reduce_fusion.3
  115.5 1.1 fusion.65
  116.6 2.2 %fusion.67 = f32[1,1536,64]{1,2,0:T(8,128)S(1)} fusion(f32[1024,1536]{1,0:T(8,128)S(1)} %get-tuple-element.181, f32[1536]{0:T(1024)S(1)} %get-tuple-element.182, f32[1,1536,64]{1,2,0:T(8,128)S(1)} %get-tuple-element.196, f32[1536]{0:T(1024)S(1)} %get-tuple-element.183, pred[]{:T(512)S(6)} %compare.14, ...), kind=kOutput, calls=%fused_computation.6.clone.1 | convolution fusion | flops 206340096 | bytes 7221253 | tf_op jit(solution)/shard_map/while/body/eval_jaxpr/dot_general | solution.py:111
  118.8 1.0 multiply_reduce_fusion.3
  119.9 1.1 fusion.65
  121.0 2.2 %fusion.67 = f32[1,1536,64]{1,2,0:T(8,128)S(1)} fusion(f32[1024,1536]{1,0:T(8,128)S(1)} %get-tuple-element.181, f32[1536]{0:T(1024)S(1)} %get-tuple-element.182, f32[1,1536,64]{1,2,0:T(8,128)S(1)} %get-tuple-element.196, f32[1536]{0:T(1024)S(1)} %get-tuple-element.183, pred[]{:T(512)S(6)} %compare.14, ...), kind=kOutput, calls=%fused_computation.6.clone.1 | convolution fusion | flops 206340096 | bytes 7221253 | tf_op jit(solution)/shard_map/while/body/eval_jaxpr/dot_general | solution.py:111
  123.1 1.0 multiply_reduce_fusion.3
  124.2 1.1 fusion.65
  125.3 2.2 %fusion.67 = f32[1,1536,64]{1,2,0:T(8,128)S(1)} fusion(f32[1024,1536]{1,0:T(8,128)S(1)} %get-tuple-element.181, f32[1536]{0:T(1024)S(1)} %get-tuple-element.182, f32[1,1536,64]{1,2,0:T(8,128)S(1)} %get-tuple-element.196, f32[1536]{0:T(1024)S(1)} %get-tuple-element.183, pred[]{:T(512)S(6)} %compare.14, ...), kind=kOutput, calls=%fused_computation.6.clone.1 | convolution fusion | flops 206340096 | bytes 7221253 | tf_op jit(solution)/shard_map/while/body/eval_jaxpr/dot_general | solution.py:111
  127.5 1.0 multiply_reduce_fusion.3
  128.6 1.1 fusion.65
  129.7 2.2 %fusion.67 = f32[1,1536,64]{1,2,0:T(8,128)S(1)} fusion(f32[1024,1536]{1,0:T(8,128)S(1)} %get-tuple-element.181, f32[1536]{0:T(1024)S(1)} %get-tuple-element.182, f32[1,1536,64]{1,2,0:T(8,128)S(1)} %get-tuple-element.196, f32[1536]{0:T(1024)S(1)} %get-tuple-element.183, pred[]{:T(512)S(6)} %compare.14, ...), kind=kOutput, calls=%fused_computation.6.clone.1 | convolution fusion | flops 206340096 | bytes 7221253 | tf_op jit(solution)/shard_map/while/body/eval_jaxpr/dot_general | solution.py:111
  131.9 1.0 multiply_reduce_fusion.3
  133.0 1.1 fusion.65
  134.1 2.2 %fusion.67 = f32[1,1536,64]{1,2,0:T(8,128)S(1)} fusion(f32[1024,1536]{1,0:T(8,128)S(1)} %get-tuple-element.181, f32[1536]{0:T(1024)S(1)} %get-tuple-element.182, f32[1,1536,64]{1,2,0:T(8,128)S(1)} %get-tuple-element.196, f32[1536]{0:T(1024)S(1)} %get-tuple-element.183, pred[]{:T(512)S(6)} %compare.14, ...), kind=kOutput, calls=%fused_computation.6.clone.1 | convolution fusion | flops 206340096 | bytes 7221253 | tf_op jit(solution)/shard_map/while/body/eval_jaxpr/dot_general | solution.py:111
  136.3 1.0 multiply_reduce_fusion.3
  137.4 1.1 fusion.65
  138.5 2.2 %fusion.67 = f32[1,1536,64]{1,2,0:T(8,128)S(1)} fusion(f32[1024,1536]{1,0:T(8,128)S(1)} %get-tuple-element.181, f32[1536]{0:T(1024)S(1)} %get-tuple-element.182, f32[1,1536,64]{1,2,0:T(8,128)S(1)} %get-tuple-element.196, f32[1536]{0:T(1024)S(1)} %get-tuple-element.183, pred[]{:T(512)S(6)} %compare.14, ...), kind=kOutput, calls=%fused_computation.6.clone.1 | convolution fusion | flops 206340096 | bytes 7221253 | tf_op jit(solution)/shard_map/while/body/eval_jaxpr/dot_general | solution.py:111
  140.8 0.2 copy.21
  141.0 0.3 reshape_transpose_reshape.4
  141.3 1.7 convolution_convert_fusion
  143.1 0.2 reshape.432
  143.3 0.7 copy.22
  144.0 24.2 %reduce-scatter.2.cloned.1.call-done = bf16[96,2048]{1,0:T(8,128)(2,1)} async-done(((bf16[384,2048]{1,0:T(8,128)(2,1)}), bf16[96,2048]{1,0:T(8,128)(2,1)}) %reduce-scatter.2.cloned.1.call-update) | async-done | bytes 393232 | tf_op jit(solution)/shard_map/reduce_scatter | solution.py:160
  (61 shorter events, 1.2 us)
Async XLA Ops:
  7.2 134.1 %copy-start = (bf16[256,2048]{1,0:T(8,128)(2,1)S(1)}, bf16[256,2048]{1,0:T(8,128)(2,1)}, u32[]{:S(2)}) copy-start(bf16[256,2048]{1,0:T(8,128)(2,1)} %param.13) | copy-start | bytes 3145732
  9.6 4.6 %copy-start.4 = (bf16[1,64]{1,0:T(2,128)(2,1)S(1)}, bf16[1,64]{1,0:T(2,128)(2,1)}, u32[]{:S(2)}) copy-start(bf16[1,64]{1,0:T(2,128)(2,1)} %param.15) | copy-start | bytes 388
  9.6 25.3 %copy-start.1 = (bf16[2048,64]{0,1:T(8,128)(2,1)S(1)}, bf16[2048,64]{0,1:T(8,128)(2,1)}, u32[]{:S(2)}) copy-start(bf16[2048,64]{0,1:T(8,128)(2,1)} %param.12) | copy-start | bytes 786436
  9.6 25.2 %all-to-all-start = ((bf16[4,96,2048]{2,1,0:T(8,128)(2,1)}), bf16[4,96,2048]{2,1,0:T(8,128)(2,1)S(1)}, u32[]{:S(2)}, u32[]{:S(2)}) async-start(bf16[4,96,2048]{2,1,0:T(8,128)(2,1)} %broadcast_in_dim.11), calls=%async_computation | async-start | bytes 3145728 | tf_op jit(solution)/shard_map/all_to_all | solution.py:22
  14.1 21.3 %copy-start.2 = (bf16[2048,64]{0,1:T(8,128)(2,1)S(1)}, bf16[2048,64]{0,1:T(8,128)(2,1)}, u32[]{:S(2)}) copy-start(bf16[2048,64]{0,1:T(8,128)(2,1)} %param.11) | copy-start | bytes 786436
  14.1 70.3 %all-gather.2.cloned.1.call-start = ((), (), s32[]{:S(2)}) async-start(), calls=%async_computation.2 | async-start | bytes 3244032 | tf_op jit(solution)/shard_map/all_gather | solution.py:34
  35.5 1.8 %copy-start.3 = (bf16[4,64]{1,0:T(4,128)(2,1)S(1)}, bf16[4,64]{1,0:T(4,128)(2,1)}, u32[]{:S(2)}) copy-start(bf16[4,64]{1,0:T(4,128)(2,1)} %param.14) | copy-start | bytes 1540
  37.1 131.1 %reduce-scatter.2.cloned.1.call-start = ((), (), s32[]{:S(2)}) async-start(), calls=%async_computation.3 | async-start | bytes 1966080 | tf_op jit(solution)/shard_map/reduce_scatter | solution.py:160
Sparse Core Ops, SparseCore 0:
  37.3 47.1 all-gather.1
  143.2 24.9 reduce-scatter.1
where the time goes:
time: 176 us; the launch traced here: 175 us
  waiting for transfers between devices  88.1 us (50%)
  matrix products  43.3 us (25%)
  other arithmetic  15.8 us (9%)
  between operations  14.3 us (8%)
  local copies, waits for them, and re-layouts  8.47 us (5%)
  starting transfers between devices  4.58 us (3%)
    all_gather x1, waiting for transfers between devices, side_by_side(): out = lax.all_gather(both, axis, axis=dim, tiled=True)  43.2 us
    dot_general x12, matrix products, inner(): lax.dot_general(expo.astype(jnp.bfloat16), value_block, (((2,), (0,)), ((...  26 us
    reduce_scatter x1, waiting for transfers between devices, body(): lax.psum_scatter(jnp.dot(attended, out_weight, preferred_element_type=jnp...  24.2 us
    all_to_all x1, waiting for transfers between devices, copy_for_each(): lax.all_to_all(jnp.broadcast_to(array[None], (count, *array.shape)), axis...  20.7 us
    reduce_sum x12, other arithmetic, inner(): total = total * factor + jnp.sum(expo, axis=-1)  12.8 us
    dot_general x12, matrix products, inner(): lax.dot_general(grouped, key_block, (((2,), (2,)), ((0,), (1,))), preferr...  12.4 us
    all_to_all x1, starting transfers between devices, copy_for_each(): lax.all_to_all(jnp.broadcast_to(array[None], (count, *array.shape)), axis...  4.54 us
  transfers between devices with their start and end apart: 3, of which 3 were waited for; matrix products, arithmetic and copies ran while one was open for 3% of the time, Pallas kernels for 0%

commit v1 on v0

v1 whole, which is shorter than its diff:
```python
import functools
import math

import jax
import jax.numpy as jnp
from jax import lax
from jax.experimental import pallas as pl
from jax.experimental.pallas import tpu as pltpu
from jax.sharding import PartitionSpec as P

MESH = pl.DeviceIdType.MESH
F32 = jnp.float32
BF16 = jnp.bfloat16
NZ, NY, NC, NX = 4, 4, 2, 4
BLK = 96
HALF = 48
D = 2048
HD = 64
HEADS = 4
GRID_W = 64
STAGE_Q = HEADS * BLK
NQ = 4 * STAGE_Q
KC = NY * NC * BLK
QT = 768
VROWS = 80
LOG2E = 1.4426950408889634
LN2 = 0.6931471805599453
OUT_ROWS = 256


def lanes(shape):
    return lax.broadcasted_iota(jnp.int32, shape, 1)


def rows(shape):
    return lax.broadcasted_iota(jnp.int32, shape, 0)


def kernel(
    tok_hbm, wq_hbm, wk_hbm, wv_hbm, wo_hbm, qg_ref, kg_ref,
    out_ref, log_ref,
    toks, wq, wk, wv, wkv, wo, perm, ones, gains, q_rows, kv, vT, sbuf, mnew, acc, mref,
    att_buf, att_in, lrows, local_sem, send_sem, tok_sem, p1_sem, p2_sem, sib_sem, wo_sem, wsib_sem, att_sem,
):
    sp = lax.axis_index("sp")
    tp = lax.axis_index("tp")
    c = lax.rem(sp, 2)
    y = lax.rem(sp // 2, 4)
    z = sp // 8

    def at_zy(zz, yy):
        return ((zz * NY + yy) * NC + c, tp)

    right, left, far = lax.rem(tp + 1, 4), lax.rem(tp + 3, 4), lax.rem(tp + 2, 4)
    sibling = (sp + 1 - 2 * c, tp)
    z_peers = [at_zy(lax.rem(z + d, 4), y) for d in (1, 2, 3)]
    y_peers = [at_zy(z, lax.rem(y + d, 4)) for d in (1, 2, 3)]
    owner = [tp, left, right, far]

    copies = [
        pltpu.make_async_copy(src, dst, local_sem.at[i])
        for i, (src, dst) in enumerate(
            [(tok_hbm, toks.at[0]), (wk_hbm, wk), (wv_hbm, wv), (wq_hbm, wq), (wo_hbm, wo.at[0])]
        )
    ]
    for copy in copies:
        copy.start()

    barrier = pltpu.get_barrier_semaphore()
    peers = [(sp, right), (sp, left), (sp, far), sibling] + z_peers + y_peers
    for peer in peers:
        pl.semaphore_signal(barrier, inc=1, device_id=peer, device_id_type=MESH)

    sends = []

    def send(src, dst, recv, peer):
        copy = pltpu.make_async_remote_copy(
            src_ref=src, dst_ref=dst, send_sem=send_sem.at[len(sends)], recv_sem=recv,
            device_id=peer, device_id_type=MESH,
        )
        sends.append(copy)
        copy.start()
        return copy

    pl.semaphore_wait(barrier, len(peers))
    copies[0].wait()

    halves = (pl.ds(0, HALF), pl.ds(HALF, HALF))
    tok_r, tok_l = [None, None], [None, None]
    for i in (0, 1):
        tok_r[i] = send(toks.at[0, halves[i]], toks.at[1, halves[i]], tok_sem.at[0, i], (sp, right))
        tok_l[1 - i] = send(
            toks.at[0, halves[1 - i]], toks.at[2, halves[1 - i]], tok_sem.at[1, 1 - i], (sp, left)
        )

    i2, j2 = rows((128, 128)), lanes((128, 128))
    lower = (j2 & 31) < 16
    perm[...] = jnp.where(
        lower & (i2 == j2 + 16), -1.0, jnp.where((~lower) & (i2 == j2 - 16), 1.0, 0.0)
    ).astype(BF16)
    ones[...] = jnp.where((i2 // 64) == (j2 // 64), 1.0 / 64.0, 0.0).astype(BF16)
    qg = qg_ref[...].astype(F32)
    kg = kg_ref[...].astype(F32)
    lane1 = lanes((8, 128))
    for g in range(3):
        if g < 2:
            pair = jnp.concatenate([qg[2 * g : 2 * g + 1], qg[2 * g + 1 : 2 * g + 2]], axis=1)
            pair = pair * (HD ** (-0.5) * LOG2E)
        else:
            pair = jnp.concatenate([kg, kg], axis=1)
        pair = jnp.broadcast_to(pair, (8, 128))
        gains[2 * g] = pair
        gains[2 * g + 1] = jnp.where((lane1 & 31) < 16, pltpu.roll(pair, 112, 1), pltpu.roll(pair, 16, 1))

    copies[1].wait()
    copies[2].wait()
    wkv[...] = jnp.concatenate([wk[...], wv[...]], axis=1)
    copies[3].wait()

    lane = lanes((BLK, 128))
    inside = lane & 63
    exponent = (inside & 15).astype(F32) * (-math.log(10000.0) / 16.0)
    freq = jnp.exp(exponent)
    zslot = z

    def project(s):
        place = sp * 384 + owner[s] * BLK + rows((BLK, 128))
        grid_row = (place >> 6).astype(F32)
        grid_col = (place & 63).astype(F32)
        angle = jnp.where(inside < 32, grid_row, grid_col) * freq
        cosine, sine = jnp.cos(angle), jnp.sin(angle)

        def prepare(raw, g):
            value = raw.astype(F32)
            turned = jnp.dot(raw, perm[...], preferred_element_type=F32)
            square = value * value
            high = square.astype(BF16)
            low = (square - high.astype(F32)).astype(BF16)
            mean = jnp.dot(high, ones[...], preferred_element_type=F32) + jnp.dot(
                low, ones[...], preferred_element_type=F32
            )
            inverse = lax.rsqrt(mean + 1e-6)
            return inverse * (
                value * gains[2 * g, 0:1] * cosine + turned * gains[2 * g + 1, 0:1] * sine
            )

        x = toks[s]
        raw = jnp.dot(x, wkv[...], preferred_element_type=F32).astype(BF16)
        slab = jnp.where(lane < 64, prepare(raw, 2), raw.astype(F32))
        kv[4 * s + zslot, y, c] = slab.astype(BF16)
        raw = jnp.dot(x, wq[...], preferred_element_type=F32).astype(BF16)
        for g in range(2):
            done = prepare(raw[:, 128 * g : 128 * g + 128], g)
            q_rows[s, 2 * g] = jnp.where(lane < 64, done, 0.0).astype(BF16)
            q_rows[s, 2 * g + 1] = jnp.where(lane < 64, pltpu.roll(done, 64, 1), 0.0).astype(BF16)

    def phase1(s):
        a = kv.at[4 * s + z, y, c, halves[0]]
        b = kv.at[4 * s + z, y, c, halves[1]]
        first = [send(a, a, p1_sem.at[s, 0, d], z_peers[d]) for d in range(3)]
        return first + [send(b, b, p1_sem.at[s, 1, d], y_peers[d]) for d in range(3)]

    def phase2(s):
        a = kv.at[pl.ds(4 * s, 4), y, c, halves[0]]
        b = kv.at[4 * s + z, :, c, halves[1]]
        first = [send(a, a, p2_sem.at[s, 0, d], y_peers[d]) for d in range(3)]
        return first + [send(b, b, p2_sem.at[s, 1, d], z_peers[d]) for d in range(3)]

    def share(s):
        a = kv.at[pl.ds(4 * s, 4), :, c]
        return [send(a, a, sib_sem.at[s], sibling)]

    def arrive(group):
        for copy in group:
            copy.wait_recv()

    project(0)
    one = {0: phase1(0)}
    two, sib = {}, {}
    arrive([tok_r[0]])
    tok_fr = send(toks.at[1, halves[0]], toks.at[3, halves[0]], tok_sem.at[2, 0], (sp, right))
    arrive([tok_l[1]])
    tok_fl = send(toks.at[2, halves[1]], toks.at[3, halves[1]], tok_sem.at[2, 1], (sp, left))
    arrive(one[0])
    two[0] = phase2(0)
    arrive(two[0])
    sib[0] = share(0)
    arrive([tok_r[1]])
    project(1)
    one[1] = phase1(1)
    arrive([tok_l[0]])
    project(2)
    one[2] = phase1(2)
    arrive(one[1])
    two[1] = phase2(1)
    arrive(one[2])
    two[2] = phase2(2)
    arrive([tok_fr, tok_fl])
    copies[4].wait()
    wo_half = OUT_ROWS // 4
    base = c * (OUT_ROWS // 2)
    wparts = [pl.ds(pl.multiple_of(base + k * wo_half, wo_half), wo_half) for k in (0, 1)]
    wo_r, wo_l = [None, None], [None, None]
    for i in (0, 1):
        wo_r[i] = send(wo.at[0, wparts[i]], wo.at[1, wparts[i]], wo_sem.at[0, i], (sp, right))
        wo_l[1 - i] = send(
            wo.at[0, wparts[1 - i]], wo.at[2, wparts[1 - i]], wo_sem.at[1, 1 - i], (sp, left)
        )
    project(3)
    one[3] = phase1(3)
    arrive(two[1])
    sib[1] = share(1)
    arrive(two[2])
    sib[2] = share(2)
    arrive(one[3])
    two[3] = phase2(3)
    arrive(two[3])
    sib[3] = share(3)
    for s in range(4):
        arrive(sib[s])

    acc[...] = jnp.zeros_like(acc)
    mref[...] = jnp.full_like(mref, -1e30)
    nt = NQ // QT

    def keys_of(n):
        return kv[n].reshape(KC, 128)

    def scores(n, t):
        q = q_rows[pl.ds(t * (QT // STAGE_Q), QT // STAGE_Q)].reshape(QT, 128)
        s = lax.dot_general(keys_of(n), q, (((1,), (1,)), ((), ())), preferred_element_type=F32)
        sbuf[t % 2] = s
        mnew[t % 2, 0:1] = jnp.max(s, axis=0, keepdims=True)

    def make_step(total):
        def step(n, carry):
            following = lax.rem(n + 1, total)
            flipped = keys_of(n).T
            vT[0:64] = flipped[64:128]
            values = vT[...]
            for t in range(nt):
                cols = pl.ds(t * QT, QT)
                if t + 1 < nt:
                    scores(n, t + 1)
                else:
                    scores(following, 0)
                s = sbuf[t % 2]
                old = mref[0:1, cols]
                new = jnp.maximum(old, mnew[t % 2, 0:1])
                weights = jnp.exp2(s - new).astype(BF16)
                factor = jnp.exp2(old - new)
                acc[:, cols] = acc[:, cols] * factor + jnp.dot(
                    values, weights, preferred_element_type=F32
                )
                mref[0:1, cols] = new
            return carry

        return step

    vT[64:VROWS] = jnp.ones((VROWS - 64, KC), BF16)
    scores(0, 0)
    step = make_step(16)
    lax.fori_loop(0, 10, step, 0)
    arrive([wo_r[0]])
    wo_fr = send(wo.at[1, wparts[0]], wo.at[3, wparts[0]], wo_sem.at[2, 0], (sp, right))
    arrive([wo_l[1]])
    wo_fl = send(wo.at[2, wparts[1]], wo.at[3, wparts[1]], wo_sem.at[2, 1], (sp, left))
    arrive([wo_r[1], wo_l[0]])
    whole = pl.ds(pl.multiple_of(base, OUT_ROWS // 2), OUT_ROWS // 2)
    wsib = [send(wo.at[k, whole], wo.at[k, whole], wsib_sem.at[k - 1], sibling) for k in (1, 2)]
    lax.fori_loop(10, 16, step, 0)

    def finish(s):
        part = acc[:, s * STAGE_Q : (s + 1) * STAGE_Q]
        o = (part[0:64] / part[64:65]).T
        for g in range(2):
            att_buf[s, :, 128 * g : 128 * g + 128] = jnp.concatenate(
                [o[2 * g * BLK : (2 * g + 1) * BLK], o[(2 * g + 1) * BLK : (2 * g + 2) * BLK]], axis=1
            ).astype(BF16)

    atts = []
    for s in (3, 1, 2):
        finish(s)
        atts.append(send(att_buf.at[s], att_in.at[s - 1], att_sem.at[s - 1], (sp, owner[s])))
    finish(0)
    arrive([wo_fr, wo_fl])
    wsib.append(send(wo.at[3, whole], wo.at[3, whole], wsib_sem.at[2], sibling))

    logs = (mref[0:1] + jnp.log2(acc[64:65])) * LN2
    tall = jnp.broadcast_to(logs, (128, NQ)).T
    for s in range(4):
        at = pl.ds(pl.multiple_of(owner[s] * BLK, BLK), BLK)
        mixed = jnp.zeros((BLK, 128), F32)
        for h in range(HEADS):
            start = s * STAGE_Q + h * BLK
            mixed = jnp.where(lane == h, tall[start : start + BLK], mixed)
        lrows[at] = mixed
    log_ref[...] = lrows[...].T[0:HEADS]

    arrive(wsib)
    arrive(atts)
    pairs = [(att_buf[0], 0), (att_in[0], 2), (att_in[1], 1), (att_in[2], 3)]
    width = 512
    for n in range(D // width):
        cols = pl.ds(n * width, width)
        total = jnp.zeros((BLK, width), F32)
        for value, slot in pairs:
            total = total + jnp.dot(value, wo[slot, :, cols], preferred_element_type=F32)
        out_ref[:, cols] = total.astype(BF16)

    for copy in sends:
        copy.wait_send()


def body(tokens, query_weight, key_weight, value_weight, out_weight, query_gain, key_gain):
    any_spec = pl.BlockSpec(memory_space=pl.ANY)
    vmem = pl.BlockSpec(memory_space=pltpu.VMEM)
    dma = pltpu.SemaphoreType.DMA
    return pl.pallas_call(
        kernel,
        out_shape=(
            jax.ShapeDtypeStruct((BLK, D), BF16),
            jax.ShapeDtypeStruct((HEADS, 4 * BLK), F32),
        ),
        in_specs=[any_spec] * 5 + [vmem] * 2,
        out_specs=(vmem, vmem),
        scratch_shapes=[
            pltpu.VMEM((4, BLK, D), BF16),
            pltpu.VMEM((D, 256), BF16),
            pltpu.VMEM((D, 64), BF16),
            pltpu.VMEM((D, 64), BF16),
            pltpu.VMEM((D, 128), BF16),
            pltpu.VMEM((4, OUT_ROWS, D), BF16),
            pltpu.VMEM((128, 128), BF16),
            pltpu.VMEM((128, 128), BF16),
            pltpu.VMEM((6, 8, 128), F32),
            pltpu.VMEM((4, HEADS, BLK, 128), BF16),
            pltpu.VMEM((16, NY, NC, BLK, 128), BF16),
            pltpu.VMEM((VROWS, KC), BF16),
            pltpu.VMEM((2, KC, QT), F32),
            pltpu.VMEM((2, 8, QT), F32),
            pltpu.VMEM((VROWS, NQ), F32),
            pltpu.VMEM((8, NQ), F32),
            pltpu.VMEM((4, BLK, 256), BF16),
            pltpu.VMEM((3, BLK, 256), BF16),
            pltpu.VMEM((4 * BLK, 128), F32),
            dma((5,)),
            dma((80,)),
            dma((3, 2)),
            dma((4, 2, 3)),
            dma((4, 2, 3)),
            dma((4,)),
            dma((3, 2)),
            dma((3,)),
            dma((3,)),
        ],
        compiler_params=pltpu.CompilerParams(
            collective_id=0, has_side_effects=True, vmem_limit_bytes=60 * 2**20
        ),
    )(tokens, query_weight, key_weight, value_weight, out_weight, query_gain, key_gain)


def solution(mesh):
    return jax.shard_map(
        body,
        mesh=mesh,
        in_specs=(
            P(("sp", "tp"), None),
            P(None, "tp"),
            P(None, "tp"),
            P(None, "tp"),
            P("tp", None),
            P("tp", None),
            P("tp", None),
        ),
        out_specs=(P(("sp", "tp"), None), P("tp", "sp")),
        check_vma=False,
    )
```

time: 176 us -> 70.4 us (0.40)
  the two profiles are of different devices: /device:TPU:0 before, /device:TPU:1 now
where the time goes in v1:
time: 70.4 us; the launch traced here: 70.2 us
  Pallas kernels  64.2 us (91%)
  local copies, waits for them, and re-layouts  5.37 us (8%)
    pallas_call x1, Pallas kernels, body(): pl.pallas_call(kernel, out_shape=(jax.ShapeDtypeStruct((BLK, D), BF16), j...  64.2 us
    unnamed x8, local copies, waits for them, and re-layouts  5.37 us

profile of v1, /device:TPU:1, one launch (start us, length us, event | category | flops | bytes accessed | tf_op | source)
XLA Modules:
  0.0 70.2 jit_solution(5029041893094338691)
XLA Ops:
  0.6 0.0 copy-start
  0.6 2.0 %copy.9.wk_hbm = bf16[2048,64]{1,0:T(8,128)(2,1)} copy(bf16[2048,64]{0,1:T(8,128)(2,1)} %param.9) | data formatting | bytes 524288 | tf_op args[2]
  2.6 0.0 copy-done
  2.6 1.0 %copy.10.wv_hbm = bf16[2048,64]{1,0:T(8,128)(2,1)} copy(bf16[2048,64]{0,1:T(8,128)(2,1)S(1)} %copy-done) | data formatting | bytes 524288 | tf_op args[3]
  3.6 64.2 %shard_map.86 = (bf16[96,2048]{1,0:T(8,128)(2,1)}, f32[4,384]{1,0:T(4,128)}) custom-call(bf16[96,2048]{1,0:T(8,128)(2,1)} %tok_hbm.1, bf16[2048,256]{1,0:T(8,128)(2,1)} %wq_hbm.1, bf16[2048,64]{1,0:T(8,128)(2,1)} %copy.9.wk_hbm, bf16[2048,64]{1,0:T(8,128)(2,1)} %copy.10.wv_hbm, bf16[256,2048]{1,0:T(8,128)(2,1)} %wo_hbm.1, bf16[4,64]{1,0:T(4,128)(2,1)} %qg_ref.1, ...), custom_call_target="tpu_custom_call" | custom-call | tf_op jit(solution)/shard_map/pallas_call | solution.py:319
  67.8 0.0 copy-start.1
  67.9 1.8 %copy.13 = bf16[96,2048]{1,0:T(8,128)(2,1)} copy(bf16[96,2048]{1,0:T(8,128)(2,1)} %get-tuple-element.4) | data formatting | bytes 786432
  69.6 0.0 copy-done.1
  69.6 0.6 copy.14
Async XLA Ops:
  0.6 2.0 %copy-start = (bf16[2048,64]{0,1:T(8,128)(2,1)S(1)}, bf16[2048,64]{0,1:T(8,128)(2,1)}, u32[]{:S(2)}) copy-start(bf16[2048,64]{0,1:T(8,128)(2,1)} %param.10) | copy-start | bytes 786436
  67.8 1.8 %copy-start.1 = (f32[4,384]{1,0:T(4,128)S(1)}, f32[4,384]{1,0:T(4,128)}, u32[]{:S(2)}) copy-start(f32[4,384]{1,0:T(4,128)} %get-tuple-element.5) | copy-start | bytes 18436

commit v2 on v1

--- a/solution.py
+++ b/solution.py
@@ -39,7 +39,7 @@
 def kernel(
     tok_hbm, wq_hbm, wk_hbm, wv_hbm, wo_hbm, qg_ref, kg_ref,
     out_ref, log_ref,
-    toks, wq, wk, wv, wkv, wo, perm, ones, gains, q_rows, kv, vT, sbuf, mnew, acc, mref,
+    toks, wq, wkv, wo, perm, ones, gains, q_rows, kv, vT, sbuf, mnew, acc, mref,
     att_buf, att_in, lrows, local_sem, send_sem, tok_sem, p1_sem, p2_sem, sib_sem, wo_sem, wsib_sem, att_sem,
 ):
     sp = lax.axis_index("sp")
@@ -60,7 +60,10 @@
     copies = [
         pltpu.make_async_copy(src, dst, local_sem.at[i])
         for i, (src, dst) in enumerate(
-            [(tok_hbm, toks.at[0]), (wk_hbm, wk), (wv_hbm, wv), (wq_hbm, wq), (wo_hbm, wo.at[0])]
+            [
+                (tok_hbm, toks.at[0]), (wk_hbm, wkv.at[pl.ds(0, HD)]), (wv_hbm, wkv.at[pl.ds(HD, HD)]),
+                (wq_hbm, wq), (wo_hbm, wo.at[0]),
+            ]
         )
     ]
     for copy in copies:
@@ -81,17 +84,6 @@
         sends.append(copy)
         copy.start()
         return copy
-
-    pl.semaphore_wait(barrier, len(peers))
-    copies[0].wait()
-
-    halves = (pl.ds(0, HALF), pl.ds(HALF, HALF))
-    tok_r, tok_l = [None, None], [None, None]
-    for i in (0, 1):
-        tok_r[i] = send(toks.at[0, halves[i]], toks.at[1, halves[i]], tok_sem.at[0, i], (sp, right))
-        tok_l[1 - i] = send(
-            toks.at[0, halves[1 - i]], toks.at[2, halves[1 - i]], tok_sem.at[1, 1 - i], (sp, left)
-        )
 
     i2, j2 = rows((128, 128)), lanes((128, 128))
     lower = (j2 & 31) < 16
@@ -112,10 +104,17 @@
         gains[2 * g] = pair
         gains[2 * g + 1] = jnp.where((lane1 & 31) < 16, pltpu.roll(pair, 112, 1), pltpu.roll(pair, 16, 1))
 
-    copies[1].wait()
-    copies[2].wait()
-    wkv[...] = jnp.concatenate([wk[...], wv[...]], axis=1)
-    copies[3].wait()
+    pl.semaphore_wait(barrier, len(peers))
+    copies[0].wait()
+    halves = (pl.ds(0, HALF), pl.ds(HALF, HALF))
+    tok_r, tok_l = [None, None], [None, None]
+    for i in (0, 1):
+        tok_r[i] = send(toks.at[0, halves[i]], toks.at[1 + i, halves[0]], tok_sem.at[0, i], (sp, right))
+        tok_l[1 - i] = send(
+            toks.at[0, halves[1 - i]], toks.at[1 + i, halves[1]], tok_sem.at[1, 1 - i], (sp, left)
+        )
+    for copy in copies[1:4]:
+        copy.wait()
 
     lane = lanes((BLK, 128))
     inside = lane & 63
@@ -124,7 +123,14 @@
     zslot = z
 
     def project(s):
-        place = sp * 384 + owner[s] * BLK + rows((BLK, 128))
+        within = rows((BLK, 128))
+        if s == 1:
+            place = jnp.where(within < HALF, left * BLK, right * BLK) + within
+        elif s == 2:
+            place = jnp.where(within < HALF, left * BLK + HALF, right * BLK - HALF) + within
+        else:
+            place = owner[s] * BLK + within
+        place = sp * 384 + place
         grid_row = (place >> 6).astype(F32)
         grid_col = (place & 63).astype(F32)
         angle = jnp.where(inside < 32, grid_row, grid_col) * freq
@@ -145,7 +151,9 @@
             )
 
         x = toks[s]
-        raw = jnp.dot(x, wkv[...], preferred_element_type=F32).astype(BF16)
+        raw = lax.dot_general(
+            x, wkv[...], (((1,), (1,)), ((), ())), preferred_element_type=F32
+        ).astype(BF16)
         slab = jnp.where(lane < 64, prepare(raw, 2), raw.astype(F32))
         kv[4 * s + zslot, y, c] = slab.astype(BF16)
         raw = jnp.dot(x, wq[...], preferred_element_type=F32).astype(BF16)
@@ -174,27 +182,79 @@
         for copy in group:
             copy.wait_recv()
 
+    acc[...] = jnp.zeros_like(acc)
+    mref[...] = jnp.full_like(mref, -1e30)
+    vT[:, HD:VROWS] = jnp.ones((2, VROWS - HD, KC), BF16)
+    per_tile = QT // STAGE_Q
+
+    def keys_of(n):
+        return kv[n].reshape(KC, 128)
+
+    def scores(n, t, slot):
+        q = q_rows[pl.ds(t * per_tile, per_tile)].reshape(QT, 128)
+        s = lax.dot_general(keys_of(n), q, (((1,), (1,)), ((), ())), preferred_element_type=F32)
+        sbuf[slot] = s
+        mnew[slot, 0:1] = jnp.max(s, axis=0, keepdims=True)
+
+    def weigh(t, slot, values):
+        cols = pl.ds(t * QT, QT)
+        old = mref[0:1, cols]
+        new = jnp.maximum(old, mnew[slot, 0:1])
+        weights = jnp.exp2(sbuf[slot] - new).astype(BF16)
+        factor = jnp.exp2(old - new)
+        acc[:, cols] = acc[:, cols] * factor + jnp.dot(values, weights, preferred_element_type=F32)
+        mref[0:1, cols] = new
+
+    def values_of(n, slot):
+        flipped = keys_of(n).T
+        vT[slot, 0:HD] = flipped[HD:128]
+        return vT[slot]
+
+    def attend(first, count, tile):
+        def step(k, carry):
+            n = first + 2 * k
+            values = values_of(n, 0)
+            scores(n + 1, tile, 1)
+            weigh(tile, 0, values)
+            values = values_of(n + 1, 1)
+            scores(first + lax.rem(2 * k + 2, count), tile, 0)
+            weigh(tile, 1, values)
+            return carry
+
+        scores(first, tile, 0)
+        lax.fori_loop(0, count // 2, step, 0)
+
+    def finish(s):
+        part = acc[:, s * STAGE_Q : (s + 1) * STAGE_Q]
+        o = (part[0:HD] / part[HD : HD + 1]).T
+        for g in range(2):
+            att_buf[s, :, 128 * g : 128 * g + 128] = jnp.concatenate(
+                [o[2 * g * BLK : (2 * g + 1) * BLK], o[(2 * g + 1) * BLK : (2 * g + 2) * BLK]], axis=1
+            ).astype(BF16)
+
     project(0)
-    one = {0: phase1(0)}
-    two, sib = {}, {}
+    one0 = phase1(0)
+    arrive(one0)
+    two0 = phase2(0)
     arrive([tok_r[0]])
     tok_fr = send(toks.at[1, halves[0]], toks.at[3, halves[0]], tok_sem.at[2, 0], (sp, right))
     arrive([tok_l[1]])
-    tok_fl = send(toks.at[2, halves[1]], toks.at[3, halves[1]], tok_sem.at[2, 1], (sp, left))
-    arrive(one[0])
-    two[0] = phase2(0)
-    arrive(two[0])
-    sib[0] = share(0)
-    arrive([tok_r[1]])
+    tok_fl = send(toks.at[1, halves[1]], toks.at[3, halves[1]], tok_sem.at[2, 1], (sp, left))
     project(1)
-    one[1] = phase1(1)
-    arrive([tok_l[0]])
+    one1 = phase1(1)
+    arrive(two0)
+    sib0 = share(0)
+    arrive(one1)
+    two1 = phase2(1)
+    arrive([tok_r[1], tok_l[0]])
     project(2)
-    one[2] = phase1(2)
-    arrive(one[1])
-    two[1] = phase2(1)
-    arrive(one[2])
-    two[2] = phase2(2)
+    one2 = phase1(2)
+    arrive(sib0)
+    attend(0, 4, 0)
+    arrive(one2)
+    two2 = phase2(2)
+    arrive(two1)
+    sib1 = share(1)
     arrive([tok_fr, tok_fl])
     copies[4].wait()
     wo_half = OUT_ROWS // 4
@@ -207,94 +267,57 @@
             wo.at[0, wparts[1 - i]], wo.at[2, wparts[1 - i]], wo_sem.at[1, 1 - i], (sp, left)
         )
     project(3)
-    one[3] = phase1(3)
-    arrive(two[1])
-    sib[1] = share(1)
-    arrive(two[2])
-    sib[2] = share(2)
-    arrive(one[3])
-    two[3] = phase2(3)
-    arrive(two[3])
-    sib[3] = share(3)
-    for s in range(4):
-        arrive(sib[s])
-
-    acc[...] = jnp.zeros_like(acc)
-    mref[...] = jnp.full_like(mref, -1e30)
-    nt = NQ // QT
-
-    def keys_of(n):
-        return kv[n].reshape(KC, 128)
-
-    def scores(n, t):
-        q = q_rows[pl.ds(t * (QT // STAGE_Q), QT // STAGE_Q)].reshape(QT, 128)
-        s = lax.dot_general(keys_of(n), q, (((1,), (1,)), ((), ())), preferred_element_type=F32)
-        sbuf[t % 2] = s
-        mnew[t % 2, 0:1] = jnp.max(s, axis=0, keepdims=True)
-
-    def make_step(total):
-        def step(n, carry):
-            following = lax.rem(n + 1, total)
-            flipped = keys_of(n).T
-            vT[0:64] = flipped[64:128]
-            values = vT[...]
-            for t in range(nt):
-                cols = pl.ds(t * QT, QT)
-                if t + 1 < nt:
-                    scores(n, t + 1)
-                else:
-                    scores(following, 0)
-                s = sbuf[t % 2]
-                old = mref[0:1, cols]
-                new = jnp.maximum(old, mnew[t % 2, 0:1])
-                weights = jnp.exp2(s - new).astype(BF16)
-                factor = jnp.exp2(old - new)
-                acc[:, cols] = acc[:, cols] * factor + jnp.dot(
-                    values, weights, preferred_element_type=F32
-                )
-                mref[0:1, cols] = new
-            return carry
-
-        return step
-
-    vT[64:VROWS] = jnp.ones((VROWS - 64, KC), BF16)
-    scores(0, 0)
-    step = make_step(16)
-    lax.fori_loop(0, 10, step, 0)
+    one3 = phase1(3)
+    arrive(sib1)
+    attend(4, 4, 0)
+    arrive(one3)
+    two3 = phase2(3)
+    arrive(two2)
+    sib2 = share(2)
+    attend(0, 8, 1)
     arrive([wo_r[0]])
     wo_fr = send(wo.at[1, wparts[0]], wo.at[3, wparts[0]], wo_sem.at[2, 0], (sp, right))
     arrive([wo_l[1]])
     wo_fl = send(wo.at[2, wparts[1]], wo.at[3, wparts[1]], wo_sem.at[2, 1], (sp, left))
+    arrive(two3)
+    sib3 = share(3)
+    arrive(sib2)
+    arrive(sib3)
+    attend(8, 8, 1)
+    finish(2)
+    finish(3)
+
+    def hand_over(s, half, slot, into, sem, peer):
+        return send(att_buf.at[s, halves[half]], att_in.at[slot, halves[into]], att_sem.at[sem], peer)
+
+    atts = [
+        hand_over(2, 0, 0, 1, 0, (sp, left)),
+        hand_over(2, 1, 1, 0, 1, (sp, right)),
+        send(att_buf.at[3], att_in.at[2], att_sem.at[2], (sp, far)),
+    ]
     arrive([wo_r[1], wo_l[0]])
     whole = pl.ds(pl.multiple_of(base, OUT_ROWS // 2), OUT_ROWS // 2)
     wsib = [send(wo.at[k, whole], wo.at[k, whole], wsib_sem.at[k - 1], sibling) for k in (1, 2)]
-    lax.fori_loop(10, 16, step, 0)
-
-    def finish(s):
-        part = acc[:, s * STAGE_Q : (s + 1) * STAGE_Q]
-        o = (part[0:64] / part[64:65]).T
-        for g in range(2):
-            att_buf[s, :, 128 * g : 128 * g + 128] = jnp.concatenate(
-                [o[2 * g * BLK : (2 * g + 1) * BLK], o[(2 * g + 1) * BLK : (2 * g + 2) * BLK]], axis=1
-            ).astype(BF16)
-
-    atts = []
-    for s in (3, 1, 2):
-        finish(s)
-        atts.append(send(att_buf.at[s], att_in.at[s - 1], att_sem.at[s - 1], (sp, owner[s])))
+    attend(8, 8, 0)
+    finish(1)
+    atts.append(hand_over(1, 0, 0, 0, 3, (sp, left)))
+    atts.append(hand_over(1, 1, 1, 1, 4, (sp, right)))
     finish(0)
     arrive([wo_fr, wo_fl])
     wsib.append(send(wo.at[3, whole], wo.at[3, whole], wsib_sem.at[2], sibling))
 
     logs = (mref[0:1] + jnp.log2(acc[64:65])) * LN2
     tall = jnp.broadcast_to(logs, (128, NQ)).T
-    for s in range(4):
-        at = pl.ds(pl.multiple_of(owner[s] * BLK, BLK), BLK)
-        mixed = jnp.zeros((BLK, 128), F32)
+    places = [
+        (0, tp * BLK), (HALF, tp * BLK + HALF), (0, left * BLK), (HALF, right * BLK + HALF),
+        (0, left * BLK + HALF), (HALF, right * BLK), (0, far * BLK), (HALF, far * BLK + HALF),
+    ]
+    for k, (inner, place) in enumerate(places):
+        mixed = jnp.zeros((HALF, 128), F32)
         for h in range(HEADS):
-            start = s * STAGE_Q + h * BLK
-            mixed = jnp.where(lane == h, tall[start : start + BLK], mixed)
-        lrows[at] = mixed
+            start = (k // 2) * STAGE_Q + h * BLK + inner
+            mixed = jnp.where(lane[0:HALF] == h, tall[start : start + HALF], mixed)
+        lrows[pl.ds(pl.multiple_of(place, HALF), HALF)] = mixed
     log_ref[...] = lrows[...].T[0:HEADS]
 
     arrive(wsib)
@@ -327,16 +350,14 @@
         scratch_shapes=[
             pltpu.VMEM((4, BLK, D), BF16),
             pltpu.VMEM((D, 256), BF16),
-            pltpu.VMEM((D, 64), BF16),
-            pltpu.VMEM((D, 64), BF16),
-            pltpu.VMEM((D, 128), BF16),
+            pltpu.VMEM((128, D), BF16),
             pltpu.VMEM((4, OUT_ROWS, D), BF16),
             pltpu.VMEM((128, 128), BF16),
             pltpu.VMEM((128, 128), BF16),
             pltpu.VMEM((6, 8, 128), F32),
             pltpu.VMEM((4, HEADS, BLK, 128), BF16),
             pltpu.VMEM((16, NY, NC, BLK, 128), BF16),
-            pltpu.VMEM((VROWS, KC), BF16),
+            pltpu.VMEM((2, VROWS, KC), BF16),
             pltpu.VMEM((2, KC, QT), F32),
             pltpu.VMEM((2, 8, QT), F32),
             pltpu.VMEM((VROWS, NQ), F32),
@@ -352,12 +373,12 @@
             dma((4,)),
             dma((3, 2)),
             dma((3,)),
-            dma((3,)),
+            dma((5,)),
         ],
         compiler_params=pltpu.CompilerParams(
             collective_id=0, has_side_effects=True, vmem_limit_bytes=60 * 2**20
         ),
-    )(tokens, query_weight, key_weight, value_weight, out_weight, query_gain, key_gain)
+    )(tokens, query_weight, key_weight.T, value_weight.T, out_weight, query_gain, key_gain)
 
 
 def solution(mesh):

time: 70.4 us -> 58.2 us (0.83)
  the two profiles are of different devices: /device:TPU:1 before, /device:TPU:0 now
where the time goes in v2:
time: 58.2 us; the launch traced here: 57 us
  Pallas kernels  54 us (93%)
  local copies, waits for them, and re-layouts  2.37 us (4%)
  between operations  0.65 us (1%)
    pallas_call x1, Pallas kernels, body(): pl.pallas_call(kernel, out_shape=(jax.ShapeDtypeStruct((BLK, D), BF16), j...  54 us
    unnamed x4, local copies, waits for them, and re-layouts  2.37 us

profile of v2, /device:TPU:0, one launch (start us, length us, event | category | flops | bytes accessed | tf_op | source)
XLA Modules:
  0.0 57.0 jit_solution(2423498094576380215)
XLA Ops:
  0.6 54.0 %shard_map.86 = (bf16[96,2048]{1,0:T(8,128)(2,1)}, f32[4,384]{1,0:T(4,128)}) custom-call(bf16[96,2048]{1,0:T(8,128)(2,1)} %tok_hbm.1, bf16[2048,256]{1,0:T(8,128)(2,1)} %wq_hbm.1, bf16[64,2048]{1,0:T(8,128)(2,1)} %bitcast.2, bf16[64,2048]{1,0:T(8,128)(2,1)} %bitcast.3, bf16[256,2048]{1,0:T(8,128)(2,1)} %wo_hbm.1, bf16[4,64]{1,0:T(4,128)(2,1)} %qg_ref.1, ...), custom_call_target="tpu_custom_call" | custom-call | tf_op jit(solution)/shard_map/pallas_call | solution.py:342
  54.7 0.0 copy-start
  54.7 1.8 %copy.11 = bf16[96,2048]{1,0:T(8,128)(2,1)} copy(bf16[96,2048]{1,0:T(8,128)(2,1)} %get-tuple-element.4) | data formatting | bytes 786432
  56.4 0.0 copy-done
  56.4 0.6 %copy.12 = f32[4,384]{1,0:T(4,128)} copy(f32[4,384]{1,0:T(4,128)S(1)} %copy-done) | data formatting | bytes 12288
Async XLA Ops:
  54.7 1.8 %copy-start = (f32[4,384]{1,0:T(4,128)S(1)}, f32[4,384]{1,0:T(4,128)}, u32[]{:S(2)}) copy-start(f32[4,384]{1,0:T(4,128)} %get-tuple-element.5) | copy-start | bytes 18436

commit v3 on v2

--- a/solution.py
+++ b/solution.py
@@ -25,6 +25,9 @@
 VROWS = 80
 LOG2E = 1.4426950408889634
 LN2 = 0.6931471805599453
+ORDER = [(0, 0, r) for r in range(4)] + [(0, 1, 0), (0, 1, 1)] + [(1, 0, r) for r in range(4)]
+ORDER += [(0, 1, 2), (0, 1, 3)] + [(1, 1, r) for r in range(4)]
+ORDER += [(t, s, r) for s in (2, 3) for t in (1, 0) for r in range(4)]
 OUT_ROWS = 256
 
 
@@ -120,7 +123,6 @@
     inside = lane & 63
     exponent = (inside & 15).astype(F32) * (-math.log(10000.0) / 16.0)
     freq = jnp.exp(exponent)
-    zslot = z
 
     def project(s):
         within = rows((BLK, 128))
@@ -155,7 +157,7 @@
             x, wkv[...], (((1,), (1,)), ((), ())), preferred_element_type=F32
         ).astype(BF16)
         slab = jnp.where(lane < 64, prepare(raw, 2), raw.astype(F32))
-        kv[4 * s + zslot, y, c] = slab.astype(BF16)
+        kv[c, 4 * s + z, y] = slab.astype(BF16)
         raw = jnp.dot(x, wq[...], preferred_element_type=F32).astype(BF16)
         for g in range(2):
             done = prepare(raw[:, 128 * g : 128 * g + 128], g)
@@ -163,19 +165,19 @@
             q_rows[s, 2 * g + 1] = jnp.where(lane < 64, pltpu.roll(done, 64, 1), 0.0).astype(BF16)
 
     def phase1(s):
-        a = kv.at[4 * s + z, y, c, halves[0]]
-        b = kv.at[4 * s + z, y, c, halves[1]]
+        a = kv.at[c, 4 * s + z, y, halves[0]]
+        b = kv.at[c, 4 * s + z, y, halves[1]]
         first = [send(a, a, p1_sem.at[s, 0, d], z_peers[d]) for d in range(3)]
         return first + [send(b, b, p1_sem.at[s, 1, d], y_peers[d]) for d in range(3)]
 
     def phase2(s):
-        a = kv.at[pl.ds(4 * s, 4), y, c, halves[0]]
-        b = kv.at[4 * s + z, :, c, halves[1]]
+        a = kv.at[c, pl.ds(4 * s, 4), y, halves[0]]
+        b = kv.at[c, 4 * s + z, :, halves[1]]
         first = [send(a, a, p2_sem.at[s, 0, d], y_peers[d]) for d in range(3)]
         return first + [send(b, b, p2_sem.at[s, 1, d], z_peers[d]) for d in range(3)]
 
     def share(s):
-        a = kv.at[pl.ds(4 * s, 4), :, c]
+        a = kv.at[c, pl.ds(4 * s, 4)]
         return [send(a, a, sib_sem.at[s], sibling)]
 
     def arrive(group):
@@ -187,45 +189,45 @@
     vT[:, HD:VROWS] = jnp.ones((2, VROWS - HD, KC), BF16)
     per_tile = QT // STAGE_Q
 
-    def keys_of(n):
-        return kv[n].reshape(KC, 128)
-
-    def scores(n, t, slot):
-        q = q_rows[pl.ds(t * per_tile, per_tile)].reshape(QT, 128)
-        s = lax.dot_general(keys_of(n), q, (((1,), (1,)), ((), ())), preferred_element_type=F32)
+    def keys_of(i):
+        s, r = ORDER[i][1:]
+        core = lax.rem(c + r // 2, 2)
+        place = 4 * s + 2 * (r % 2)
+        return kv[core, place : place + 2].reshape(KC, 128)
+
+    def scores(i):
+        tile, slot = ORDER[i][0], i % 2
+        q = q_rows[tile * per_tile : (tile + 1) * per_tile].reshape(QT, 128)
+        s = lax.dot_general(keys_of(i), q, (((1,), (1,)), ((), ())), preferred_element_type=F32)
         sbuf[slot] = s
         mnew[slot, 0:1] = jnp.max(s, axis=0, keepdims=True)
 
-    def weigh(t, slot, values):
-        cols = pl.ds(t * QT, QT)
-        old = mref[0:1, cols]
+    def weigh(i):
+        tile, slot = ORDER[i][0], i % 2
+        flipped = keys_of(i).T
+        vT[slot, 0:HD] = flipped[HD:128]
+        old = mref[tile, 0:1]
         new = jnp.maximum(old, mnew[slot, 0:1])
         weights = jnp.exp2(sbuf[slot] - new).astype(BF16)
         factor = jnp.exp2(old - new)
-        acc[:, cols] = acc[:, cols] * factor + jnp.dot(values, weights, preferred_element_type=F32)
-        mref[0:1, cols] = new
-
-    def values_of(n, slot):
-        flipped = keys_of(n).T
-        vT[slot, 0:HD] = flipped[HD:128]
-        return vT[slot]
-
-    def attend(first, count, tile):
-        def step(k, carry):
-            n = first + 2 * k
-            values = values_of(n, 0)
-            scores(n + 1, tile, 1)
-            weigh(tile, 0, values)
-            values = values_of(n + 1, 1)
-            scores(first + lax.rem(2 * k + 2, count), tile, 0)
-            weigh(tile, 1, values)
-            return carry
-
-        scores(first, tile, 0)
-        lax.fori_loop(0, count // 2, step, 0)
+        acc[tile] = acc[tile] * factor + jnp.dot(vT[slot], weights, preferred_element_type=F32)
+        mref[tile, 0:1] = new
+
+    def tiles(lo, hi):
+        while lo < hi:
+            end = min(lo + 2, hi)
+
+            @pl.when(sp >= 0)
+            def _():
+                for i in range(lo, end):
+                    if i + 1 < len(ORDER):
+                        scores(i + 1)
+                    weigh(i)
+
+            lo = end
 
     def finish(s):
-        part = acc[:, s * STAGE_Q : (s + 1) * STAGE_Q]
+        part = acc[s // 2, :, (s % 2) * STAGE_Q : (s % 2 + 1) * STAGE_Q]
         o = (part[0:HD] / part[HD : HD + 1]).T
         for g in range(2):
             att_buf[s, :, 128 * g : 128 * g + 128] = jnp.concatenate(
@@ -244,17 +246,15 @@
     one1 = phase1(1)
     arrive(two0)
     sib0 = share(0)
+    scores(0)
+    tiles(0, 1)
     arrive(one1)
     two1 = phase2(1)
     arrive([tok_r[1], tok_l[0]])
     project(2)
     one2 = phase1(2)
     arrive(sib0)
-    attend(0, 4, 0)
-    arrive(one2)
-    two2 = phase2(2)
-    arrive(two1)
-    sib1 = share(1)
+    tiles(1, 3)
     arrive([tok_fr, tok_fl])
     copies[4].wait()
     wo_half = OUT_ROWS // 4
@@ -268,22 +268,32 @@
         )
     project(3)
     one3 = phase1(3)
-    arrive(sib1)
-    attend(4, 4, 0)
+    arrive(one2)
+    two2 = phase2(2)
+    arrive(two1)
+    sib1 = share(1)
+    tiles(3, 7)
     arrive(one3)
     two3 = phase2(3)
+    tiles(7, 9)
     arrive(two2)
     sib2 = share(2)
-    attend(0, 8, 1)
+    arrive(sib1)
+    tiles(9, 13)
+    arrive(two3)
+    sib3 = share(3)
+    tiles(13, 15)
     arrive([wo_r[0]])
     wo_fr = send(wo.at[1, wparts[0]], wo.at[3, wparts[0]], wo_sem.at[2, 0], (sp, right))
     arrive([wo_l[1]])
     wo_fl = send(wo.at[2, wparts[1]], wo.at[3, wparts[1]], wo_sem.at[2, 1], (sp, left))
-    arrive(two3)
-    sib3 = share(3)
     arrive(sib2)
+    tiles(15, 23)
+    arrive([wo_r[1], wo_l[0]])
+    whole = pl.ds(pl.multiple_of(base, OUT_ROWS // 2), OUT_ROWS // 2)
+    wsib = [send(wo.at[k, whole], wo.at[k, whole], wsib_sem.at[k - 1], sibling) for k in (1, 2)]
     arrive(sib3)
-    attend(8, 8, 1)
+    tiles(23, 28)
     finish(2)
     finish(3)
 
@@ -295,18 +305,18 @@
         hand_over(2, 1, 1, 0, 1, (sp, right)),
         send(att_buf.at[3], att_in.at[2], att_sem.at[2], (sp, far)),
     ]
-    arrive([wo_r[1], wo_l[0]])
-    whole = pl.ds(pl.multiple_of(base, OUT_ROWS // 2), OUT_ROWS // 2)
-    wsib = [send(wo.at[k, whole], wo.at[k, whole], wsib_sem.at[k - 1], sibling) for k in (1, 2)]
-    attend(8, 8, 0)
+    tiles(28, 31)
+    arrive([wo_fr, wo_fl])
+    wsib.append(send(wo.at[3, whole], wo.at[3, whole], wsib_sem.at[2], sibling))
+    tiles(31, 32)
     finish(1)
     atts.append(hand_over(1, 0, 0, 0, 3, (sp, left)))
     atts.append(hand_over(1, 1, 1, 1, 4, (sp, right)))
     finish(0)
-    arrive([wo_fr, wo_fl])
-    wsib.append(send(wo.at[3, whole], wo.at[3, whole], wsib_sem.at[2], sibling))
-
-    logs = (mref[0:1] + jnp.log2(acc[64:65])) * LN2
+
+    logs = jnp.concatenate(
+        [(mref[k, 0:1] + jnp.log2(acc[k, HD : HD + 1])) * LN2 for k in (0, 1)], axis=1
+    )
     tall = jnp.broadcast_to(logs, (128, NQ)).T
     places = [
         (0, tp * BLK), (HALF, tp * BLK + HALF), (0, left * BLK), (HALF, right * BLK + HALF),
@@ -356,12 +366,12 @@
             pltpu.VMEM((128, 128), BF16),
             pltpu.VMEM((6, 8, 128), F32),
             pltpu.VMEM((4, HEADS, BLK, 128), BF16),
-            pltpu.VMEM((16, NY, NC, BLK, 128), BF16),
+            pltpu.VMEM((NC, 16, NY, BLK, 128), BF16),
             pltpu.VMEM((2, VROWS, KC), BF16),
             pltpu.VMEM((2, KC, QT), F32),
             pltpu.VMEM((2, 8, QT), F32),
-            pltpu.VMEM((VROWS, NQ), F32),
-            pltpu.VMEM((8, NQ), F32),
+            pltpu.VMEM((2, VROWS, QT), F32),
+            pltpu.VMEM((2, 8, QT), F32),
             pltpu.VMEM((4, BLK, 256), BF16),
             pltpu.VMEM((3, BLK, 256), BF16),
             pltpu.VMEM((4 * BLK, 128), F32),

time: 58.2 us -> 53 us (0.911); the launches traced: 57 us -> 52.9 us
  Pallas kernels: 54 us -> 49.8 us
    pallas_call x1, Pallas kernels: 54 us -> 49.8 us  [body(): pl.pallas_call(kernel, out_shape=(jax.ShapeDtypeStruct((BLK, D), BF16), j...]
where the time goes in v3:
time: 53 us; the launch traced here: 52.9 us
  Pallas kernels  49.8 us (94%)
  local copies, waits for them, and re-layouts  2.37 us (4%)
  between operations  0.65 us (1%)
    pallas_call x1, Pallas kernels, body(): pl.pallas_call(kernel, out_shape=(jax.ShapeDtypeStruct((BLK, D), BF16), j...  49.8 us
    unnamed x4, local copies, waits for them, and re-layouts  2.37 us

profile of v3, /device:TPU:0, one launch (start us, length us, event | category | flops | bytes accessed | tf_op | source)
XLA Modules:
  0.0 52.9 jit_solution(12321101595444817657)
XLA Ops:
  0.6 49.8 %shard_map.86 = (bf16[96,2048]{1,0:T(8,128)(2,1)}, f32[4,384]{1,0:T(4,128)}) custom-call(bf16[96,2048]{1,0:T(8,128)(2,1)} %tok_hbm.1, bf16[2048,256]{1,0:T(8,128)(2,1)} %wq_hbm.1, bf16[64,2048]{1,0:T(8,128)(2,1)} %bitcast.2, bf16[64,2048]{1,0:T(8,128)(2,1)} %bitcast.3, bf16[256,2048]{1,0:T(8,128)(2,1)} %wo_hbm.1, bf16[4,64]{1,0:T(4,128)(2,1)} %qg_ref.1, ...), custom_call_target="tpu_custom_call" | custom-call | tf_op jit(solution)/shard_map/pallas_call | solution.py:352
  50.5 0.0 copy-start
  50.5 1.8 %copy.11 = bf16[96,2048]{1,0:T(8,128)(2,1)} copy(bf16[96,2048]{1,0:T(8,128)(2,1)} %get-tuple-element.4) | data formatting | bytes 786432
  52.3 0.0 copy-done
  52.3 0.6 %copy.12 = f32[4,384]{1,0:T(4,128)} copy(f32[4,384]{1,0:T(4,128)S(1)} %copy-done) | data formatting | bytes 12288
Async XLA Ops:
  50.5 1.8 %copy-start = (f32[4,384]{1,0:T(4,128)S(1)}, f32[4,384]{1,0:T(4,128)}, u32[]{:S(2)}) copy-start(f32[4,384]{1,0:T(4,128)} %get-tuple-element.5) | copy-start | bytes 18436

commit v4 on v3

--- a/solution.py
+++ b/solution.py
@@ -24,11 +24,12 @@
 QT = 768
 VROWS = 80
 LOG2E = 1.4426950408889634
+OUT_ROWS = 256
 LN2 = 0.6931471805599453
-ORDER = [(0, 0, r) for r in range(4)] + [(0, 1, 0), (0, 1, 1)] + [(1, 0, r) for r in range(4)]
-ORDER += [(0, 1, 2), (0, 1, 3)] + [(1, 1, r) for r in range(4)]
-ORDER += [(t, s, r) for s in (2, 3) for t in (1, 0) for r in range(4)]
-OUT_ROWS = 256
+ORDER = [(t, 0, r) for t in (0, 1) for r in range(4)]
+ORDER += [(t, 1, r + d) for r in (0, 2) for t in (0, 1) for d in (0, 1)]
+ORDER += [(t, 2, r + d) for r in (0, 2) for t in (1, 0) for d in (0, 1)]
+ORDER += [(t, 3, r) for t in (1, 0) for r in range(4)]
 
 
 def lanes(shape):
@@ -42,7 +43,7 @@
 def kernel(
     tok_hbm, wq_hbm, wk_hbm, wv_hbm, wo_hbm, qg_ref, kg_ref,
     out_ref, log_ref,
-    toks, wq, wkv, wo, perm, ones, gains, q_rows, kv, vT, sbuf, mnew, acc, mref,
+    toks, wq, wkv, wo, turns, total, perm, ones, gains, q_rows, kv, vT, sbuf, mnew, acc, mref,
     att_buf, att_in, lrows, local_sem, send_sem, tok_sem, p1_sem, p2_sem, sib_sem, wo_sem, wsib_sem, att_sem,
 ):
     sp = lax.axis_index("sp")
@@ -107,24 +108,12 @@
         gains[2 * g] = pair
         gains[2 * g + 1] = jnp.where((lane1 & 31) < 16, pltpu.roll(pair, 112, 1), pltpu.roll(pair, 16, 1))
 
-    pl.semaphore_wait(barrier, len(peers))
-    copies[0].wait()
-    halves = (pl.ds(0, HALF), pl.ds(HALF, HALF))
-    tok_r, tok_l = [None, None], [None, None]
-    for i in (0, 1):
-        tok_r[i] = send(toks.at[0, halves[i]], toks.at[1 + i, halves[0]], tok_sem.at[0, i], (sp, right))
-        tok_l[1 - i] = send(
-            toks.at[0, halves[1 - i]], toks.at[1 + i, halves[1]], tok_sem.at[1, 1 - i], (sp, left)
-        )
-    for copy in copies[1:4]:
-        copy.wait()
-
     lane = lanes((BLK, 128))
     inside = lane & 63
     exponent = (inside & 15).astype(F32) * (-math.log(10000.0) / 16.0)
     freq = jnp.exp(exponent)
 
-    def project(s):
+    for s in range(4):
         within = rows((BLK, 128))
         if s == 1:
             place = jnp.where(within < HALF, left * BLK, right * BLK) + within
@@ -136,31 +125,45 @@
         grid_row = (place >> 6).astype(F32)
         grid_col = (place & 63).astype(F32)
         angle = jnp.where(inside < 32, grid_row, grid_col) * freq
-        cosine, sine = jnp.cos(angle), jnp.sin(angle)
-
-        def prepare(raw, g):
-            value = raw.astype(F32)
-            turned = jnp.dot(raw, perm[...], preferred_element_type=F32)
-            square = value * value
-            high = square.astype(BF16)
-            low = (square - high.astype(F32)).astype(BF16)
-            mean = jnp.dot(high, ones[...], preferred_element_type=F32) + jnp.dot(
-                low, ones[...], preferred_element_type=F32
-            )
-            inverse = lax.rsqrt(mean + 1e-6)
-            return inverse * (
-                value * gains[2 * g, 0:1] * cosine + turned * gains[2 * g + 1, 0:1] * sine
-            )
-
-        x = toks[s]
+        turns[0, s], turns[1, s] = jnp.cos(angle), jnp.sin(angle)
+
+    pl.semaphore_wait(barrier, len(peers))
+    copies[0].wait()
+    halves = (pl.ds(0, HALF), pl.ds(HALF, HALF))
+    tok_r, tok_l = [None, None], [None, None]
+    for i in (0, 1):
+        tok_r[i] = send(toks.at[0, halves[i]], toks.at[1 + i, halves[0]], tok_sem.at[0, i], (sp, right))
+        tok_l[1 - i] = send(
+            toks.at[0, halves[1 - i]], toks.at[1 + i, halves[1]], tok_sem.at[1, 1 - i], (sp, left)
+        )
+    for copy in copies[1:4]:
+        copy.wait()
+
+    def prepare(s, raw, g):
+        value = raw.astype(F32)
+        turned = jnp.dot(raw, perm[...], preferred_element_type=F32)
+        square = value * value
+        high = square.astype(BF16)
+        low = (square - high.astype(F32)).astype(BF16)
+        mean = jnp.dot(high, ones[...], preferred_element_type=F32) + jnp.dot(
+            low, ones[...], preferred_element_type=F32
+        )
+        inverse = lax.rsqrt(mean + 1e-6)
+        return inverse * (
+            value * gains[2 * g, 0:1] * turns[0, s] + turned * gains[2 * g + 1, 0:1] * turns[1, s]
+        )
+
+    def project_keys(s):
         raw = lax.dot_general(
-            x, wkv[...], (((1,), (1,)), ((), ())), preferred_element_type=F32
+            toks[s], wkv[...], (((1,), (1,)), ((), ())), preferred_element_type=F32
         ).astype(BF16)
-        slab = jnp.where(lane < 64, prepare(raw, 2), raw.astype(F32))
+        slab = jnp.where(lane < 64, prepare(s, raw, 2), raw.astype(F32))
         kv[c, 4 * s + z, y] = slab.astype(BF16)
-        raw = jnp.dot(x, wq[...], preferred_element_type=F32).astype(BF16)
+
+    def project_queries(s):
+        raw = jnp.dot(toks[s], wq[...], preferred_element_type=F32).astype(BF16)
         for g in range(2):
-            done = prepare(raw[:, 128 * g : 128 * g + 128], g)
+            done = prepare(s, raw[:, 128 * g : 128 * g + 128], g)
             q_rows[s, 2 * g] = jnp.where(lane < 64, done, 0.0).astype(BF16)
             q_rows[s, 2 * g + 1] = jnp.where(lane < 64, pltpu.roll(done, 64, 1), 0.0).astype(BF16)
 
@@ -234,16 +237,18 @@
                 [o[2 * g * BLK : (2 * g + 1) * BLK], o[(2 * g + 1) * BLK : (2 * g + 2) * BLK]], axis=1
             ).astype(BF16)
 
-    project(0)
+    project_keys(0)
     one0 = phase1(0)
+    project_queries(0)
     arrive(one0)
     two0 = phase2(0)
     arrive([tok_r[0]])
     tok_fr = send(toks.at[1, halves[0]], toks.at[3, halves[0]], tok_sem.at[2, 0], (sp, right))
     arrive([tok_l[1]])
     tok_fl = send(toks.at[1, halves[1]], toks.at[3, halves[1]], tok_sem.at[2, 1], (sp, left))
-    project(1)
+    project_keys(1)
     one1 = phase1(1)
+    project_queries(1)
     arrive(two0)
     sib0 = share(0)
     scores(0)
@@ -251,8 +256,9 @@
     arrive(one1)
     two1 = phase2(1)
     arrive([tok_r[1], tok_l[0]])
-    project(2)
+    project_keys(2)
     one2 = phase1(2)
+    project_queries(2)
     arrive(sib0)
     tiles(1, 3)
     arrive([tok_fr, tok_fl])
@@ -266,34 +272,38 @@
         wo_l[1 - i] = send(
             wo.at[0, wparts[1 - i]], wo.at[2, wparts[1 - i]], wo_sem.at[1, 1 - i], (sp, left)
         )
-    project(3)
+    project_keys(3)
     one3 = phase1(3)
+    project_queries(3)
+    tiles(3, 5)
     arrive(one2)
     two2 = phase2(2)
     arrive(two1)
     sib1 = share(1)
-    tiles(3, 7)
+    tiles(5, 7)
     arrive(one3)
     two3 = phase2(3)
-    tiles(7, 9)
+    tiles(7, 11)
+    arrive(sib1)
+    tiles(11, 13)
     arrive(two2)
     sib2 = share(2)
-    arrive(sib1)
-    tiles(9, 13)
-    arrive(two3)
-    sib3 = share(3)
-    tiles(13, 15)
+    tiles(13, 17)
     arrive([wo_r[0]])
     wo_fr = send(wo.at[1, wparts[0]], wo.at[3, wparts[0]], wo_sem.at[2, 0], (sp, right))
     arrive([wo_l[1]])
     wo_fl = send(wo.at[2, wparts[1]], wo.at[3, wparts[1]], wo_sem.at[2, 1], (sp, left))
+    arrive(two3)
+    sib3 = share(3)
+    tiles(17, 19)
     arrive(sib2)
-    tiles(15, 23)
+    tiles(19, 23)
     arrive([wo_r[1], wo_l[0]])
     whole = pl.ds(pl.multiple_of(base, OUT_ROWS // 2), OUT_ROWS // 2)
     wsib = [send(wo.at[k, whole], wo.at[k, whole], wsib_sem.at[k - 1], sibling) for k in (1, 2)]
+    tiles(23, 25)
     arrive(sib3)
-    tiles(23, 28)
+    tiles(25, 28)
     finish(2)
     finish(3)
 
@@ -305,10 +315,10 @@
         hand_over(2, 1, 1, 0, 1, (sp, right)),
         send(att_buf.at[3], att_in.at[2], att_sem.at[2], (sp, far)),
     ]
-    tiles(28, 31)
+    tiles(28, 29)
     arrive([wo_fr, wo_fl])
     wsib.append(send(wo.at[3, whole], wo.at[3, whole], wsib_sem.at[2], sibling))
-    tiles(31, 32)
+    tiles(29, 32)
     finish(1)
     atts.append(hand_over(1, 0, 0, 0, 3, (sp, left)))
     atts.append(hand_over(1, 1, 1, 1, 4, (sp, right)))
@@ -330,16 +340,30 @@
         lrows[pl.ds(pl.multiple_of(place, HALF), HALF)] = mixed
     log_ref[...] = lrows[...].T[0:HEADS]
 
-    arrive(wsib)
-    arrive(atts)
-    pairs = [(att_buf[0], 0), (att_in[0], 2), (att_in[1], 1), (att_in[2], 3)]
     width = 512
-    for n in range(D // width):
-        cols = pl.ds(n * width, width)
-        total = jnp.zeros((BLK, width), F32)
-        for value, slot in pairs:
-            total = total + jnp.dot(value, wo[slot, :, cols], preferred_element_type=F32)
-        out_ref[:, cols] = total.astype(BF16)
+
+    def out_product(value, slot, part, first=False, last=False):
+        for n in range(D // width):
+            cols = pl.ds(n * width, width)
+            product = jnp.dot(value, wo[slot, :, cols], preferred_element_type=F32)
+            if not first:
+                product = product + total[part, cols]
+            if last:
+                out_ref[part, cols] = product.astype(BF16)
+            else:
+                total[part, cols] = product
+
+    out_product(att_buf[0], 0, pl.ds(0, BLK), first=True)
+    arrive(wsib[0:2])
+    arrive(atts[0:2])
+    out_product(att_in[1, halves[0]], 1, halves[0])
+    out_product(att_in[0, halves[1]], 2, halves[1])
+    arrive(wsib[2:3])
+    arrive(atts[2:3])
+    out_product(att_in[2], 3, pl.ds(0, BLK))
+    arrive(atts[3:5])
+    out_product(att_in[0, halves[0]], 2, halves[0], last=True)
+    out_product(att_in[1, halves[1]], 1, halves[1], last=True)
 
     for copy in sends:
         copy.wait_send()
@@ -362,6 +386,8 @@
             pltpu.VMEM((D, 256), BF16),
             pltpu.VMEM((128, D), BF16),
             pltpu.VMEM((4, OUT_ROWS, D), BF16),
+            pltpu.VMEM((2, 4, BLK, 128), F32),
+            pltpu.VMEM((BLK, D), F32),
             pltpu.VMEM((128, 128), BF16),
             pltpu.VMEM((128, 128), BF16),
             pltpu.VMEM((6, 8, 128), F32),

time: 53 us -> 50.9 us (0.960)
  Pallas kernels: 49.8 us -> 47.6 us
    pallas_call x1, Pallas kernels: 49.8 us -> 47.6 us  [body(): pl.pallas_call(kernel, out_shape=(jax.ShapeDtypeStruct((BLK, D), BF16), j...]
where the time goes in v4:
time: 50.9 us; the launch traced here: 50.6 us
  Pallas kernels  47.6 us (94%)
  local copies, waits for them, and re-layouts  2.37 us (5%)
  between operations  0.65 us (1%)
    pallas_call x1, Pallas kernels, body(): pl.pallas_call(kernel, out_shape=(jax.ShapeDtypeStruct((BLK, D), BF16), j...  47.6 us
    unnamed x4, local copies, waits for them, and re-layouts  2.37 us

profile of v4, /device:TPU:0, one launch (start us, length us, event | category | flops | bytes accessed | tf_op | source)
XLA Modules:
  0.0 50.6 jit_solution(13313681506290522806)
XLA Ops:
  0.6 47.6 %shard_map.86 = (bf16[96,2048]{1,0:T(8,128)(2,1)}, f32[4,384]{1,0:T(4,128)}) custom-call(bf16[96,2048]{1,0:T(8,128)(2,1)} %tok_hbm.1, bf16[2048,256]{1,0:T(8,128)(2,1)} %wq_hbm.1, bf16[64,2048]{1,0:T(8,128)(2,1)} %bitcast.2, bf16[64,2048]{1,0:T(8,128)(2,1)} %bitcast.3, bf16[256,2048]{1,0:T(8,128)(2,1)} %wo_hbm.1, bf16[4,64]{1,0:T(4,128)(2,1)} %qg_ref.1, ...), custom_call_target="tpu_custom_call" | custom-call | tf_op jit(solution)/shard_map/pallas_call | solution.py:376
  48.2 0.0 copy-start
  48.2 1.8 %copy.11 = bf16[96,2048]{1,0:T(8,128)(2,1)} copy(bf16[96,2048]{1,0:T(8,128)(2,1)} %get-tuple-element.4) | data formatting | bytes 786432
  50.0 0.0 copy-done
  50.0 0.6 %copy.12 = f32[4,384]{1,0:T(4,128)} copy(f32[4,384]{1,0:T(4,128)S(1)} %copy-done) | data formatting | bytes 12288
Async XLA Ops:
  48.2 1.8 %copy-start = (f32[4,384]{1,0:T(4,128)S(1)}, f32[4,384]{1,0:T(4,128)}, u32[]{:S(2)}) copy-start(f32[4,384]{1,0:T(4,128)} %get-tuple-element.5) | copy-start | bytes 18436

commit v5 on v4

--- a/solution.py
+++ b/solution.py
@@ -42,9 +42,9 @@
 
 def kernel(
     tok_hbm, wq_hbm, wk_hbm, wv_hbm, wo_hbm, qg_ref, kg_ref,
-    out_ref, log_ref,
+    out_hbm, log_hbm,
     toks, wq, wkv, wo, turns, total, perm, ones, gains, q_rows, kv, vT, sbuf, mnew, acc, mref,
-    att_buf, att_in, lrows, local_sem, send_sem, tok_sem, p1_sem, p2_sem, sib_sem, wo_sem, wsib_sem, att_sem,
+    out_ref, log_ref, att_buf, att_in, lrows, local_sem, send_sem, tok_sem, p1_sem, p2_sem, sib_sem, wo_sem, wsib_sem, att_sem,
 ):
     sp = lax.axis_index("sp")
     tp = lax.axis_index("tp")
@@ -127,6 +127,7 @@
         angle = jnp.where(inside < 32, grid_row, grid_col) * freq
         turns[0, s], turns[1, s] = jnp.cos(angle), jnp.sin(angle)
 
+    vT[:, HD:VROWS] = jnp.ones((16, VROWS - HD, KC), BF16)
     pl.semaphore_wait(barrier, len(peers))
     copies[0].wait()
     halves = (pl.ds(0, HALF), pl.ds(HALF, HALF))
@@ -189,7 +190,6 @@
 
     acc[...] = jnp.zeros_like(acc)
     mref[...] = jnp.full_like(mref, -1e30)
-    vT[:, HD:VROWS] = jnp.ones((2, VROWS - HD, KC), BF16)
     per_tile = QT // STAGE_Q
 
     def keys_of(i):
@@ -198,34 +198,41 @@
         place = 4 * s + 2 * (r % 2)
         return kv[core, place : place + 2].reshape(KC, 128)
 
-    def scores(i):
+    def scores(i, part):
         tile, slot = ORDER[i][0], i % 2
-        q = q_rows[tile * per_tile : (tile + 1) * per_tile].reshape(QT, 128)
+        q = q_rows[tile * per_tile : (tile + 1) * per_tile].reshape(QT, 128)[part]
         s = lax.dot_general(keys_of(i), q, (((1,), (1,)), ((), ())), preferred_element_type=F32)
-        sbuf[slot] = s
-        mnew[slot, 0:1] = jnp.max(s, axis=0, keepdims=True)
-
-    def weigh(i):
+        sbuf[slot, :, part] = s
+        mnew[slot, 0:1, part] = jnp.max(s, axis=0, keepdims=True)
+
+    def weigh(i, part):
         tile, slot = ORDER[i][0], i % 2
-        flipped = keys_of(i).T
-        vT[slot, 0:HD] = flipped[HD:128]
-        old = mref[tile, 0:1]
-        new = jnp.maximum(old, mnew[slot, 0:1])
-        weights = jnp.exp2(sbuf[slot] - new).astype(BF16)
-        factor = jnp.exp2(old - new)
-        acc[tile] = acc[tile] * factor + jnp.dot(vT[slot], weights, preferred_element_type=F32)
-        mref[tile, 0:1] = new
-
-    def tiles(lo, hi):
+        chunk = 4 * ORDER[i][1] + ORDER[i][2]
+        if part.start == 0 and ORDER[i][1:] not in [other[1:] for other in ORDER[:i]]:
+            flipped = keys_of(i).T
+            vT[chunk, 0:HD] = flipped[HD:128]
+        for cols in [part]:
+            old = mref[tile, 0:1, cols]
+            new = jnp.maximum(old, mnew[slot, 0:1, cols])
+            weights = jnp.exp2(sbuf[slot, :, cols] - new).astype(BF16)
+            factor = jnp.exp2(old - new)
+            acc[tile, :, cols] = acc[tile, :, cols] * factor + jnp.dot(
+                vT[chunk], weights, preferred_element_type=F32
+            )
+            mref[tile, 0:1, cols] = new
+
+    def tiles(lo, hi, parts=(0, 1)):
         while lo < hi:
             end = min(lo + 2, hi)
 
             @pl.when(sp >= 0)
             def _():
                 for i in range(lo, end):
-                    if i + 1 < len(ORDER):
-                        scores(i + 1)
-                    weigh(i)
+                    for j in parts:
+                        cols = slice(j * STAGE_Q, (j + 1) * STAGE_Q)
+                        if i + 1 < len(ORDER):
+                            scores(i + 1, cols)
+                        weigh(i, cols)
 
             lo = end
 
@@ -251,7 +258,7 @@
     project_queries(1)
     arrive(two0)
     sib0 = share(0)
-    scores(0)
+    scores(0, slice(0, QT))
     tiles(0, 1)
     arrive(one1)
     two1 = phase2(1)
@@ -315,13 +322,13 @@
         hand_over(2, 1, 1, 0, 1, (sp, right)),
         send(att_buf.at[3], att_in.at[2], att_sem.at[2], (sp, far)),
     ]
-    tiles(28, 29)
-    arrive([wo_fr, wo_fl])
-    wsib.append(send(wo.at[3, whole], wo.at[3, whole], wsib_sem.at[2], sibling))
-    tiles(29, 32)
+    tiles(28, 32, (1,))
     finish(1)
     atts.append(hand_over(1, 0, 0, 0, 3, (sp, left)))
     atts.append(hand_over(1, 1, 1, 1, 4, (sp, right)))
+    arrive([wo_fr, wo_fl])
+    wsib.append(send(wo.at[3, whole], wo.at[3, whole], wsib_sem.at[2], sibling))
+    tiles(28, 32, (0,))
     finish(0)
 
     logs = jnp.concatenate(
@@ -339,6 +346,8 @@
             mixed = jnp.where(lane[0:HALF] == h, tall[start : start + HALF], mixed)
         lrows[pl.ds(pl.multiple_of(place, HALF), HALF)] = mixed
     log_ref[...] = lrows[...].T[0:HEADS]
+    leaving = [pltpu.make_async_copy(log_ref, log_hbm, local_sem.at[5])]
+    leaving[0].start()
 
     width = 512
 
@@ -350,6 +359,12 @@
                 product = product + total[part, cols]
             if last:
                 out_ref[part, cols] = product.astype(BF16)
+                leaving.append(
+                    pltpu.make_async_copy(
+                        out_ref.at[part, cols], out_hbm.at[part, cols], local_sem.at[5 + len(leaving)]
+                    )
+                )
+                leaving[-1].start()
             else:
                 total[part, cols] = product
 
@@ -365,6 +380,8 @@
     out_product(att_in[0, halves[0]], 2, halves[0], last=True)
     out_product(att_in[1, halves[1]], 1, halves[1], last=True)
 
+    for copy in leaving:
+        copy.wait()
     for copy in sends:
         copy.wait_send()
 
@@ -380,7 +397,7 @@
             jax.ShapeDtypeStruct((HEADS, 4 * BLK), F32),
         ),
         in_specs=[any_spec] * 5 + [vmem] * 2,
-        out_specs=(vmem, vmem),
+        out_specs=(any_spec, any_spec),
         scratch_shapes=[
             pltpu.VMEM((4, BLK, D), BF16),
             pltpu.VMEM((D, 256), BF16),
@@ -393,15 +410,17 @@
             pltpu.VMEM((6, 8, 128), F32),
             pltpu.VMEM((4, HEADS, BLK, 128), BF16),
             pltpu.VMEM((NC, 16, NY, BLK, 128), BF16),
-            pltpu.VMEM((2, VROWS, KC), BF16),
+            pltpu.VMEM((16, VROWS, KC), BF16),
             pltpu.VMEM((2, KC, QT), F32),
             pltpu.VMEM((2, 8, QT), F32),
             pltpu.VMEM((2, VROWS, QT), F32),
             pltpu.VMEM((2, 8, QT), F32),
+            pltpu.VMEM((BLK, D), BF16),
+            pltpu.VMEM((HEADS, 4 * BLK), F32),
             pltpu.VMEM((4, BLK, 256), BF16),
             pltpu.VMEM((3, BLK, 256), BF16),
             pltpu.VMEM((4 * BLK, 128), F32),
-            dma((5,)),
+            dma((14,)),
             dma((80,)),
             dma((3, 2)),
             dma((4, 2, 3)),

time: 50.9 us -> 49.2 us (0.967)
  Pallas kernels: 47.6 us -> 46 us
    pallas_call x1, Pallas kernels: 47.6 us -> 46 us  [body(): pl.pallas_call(kernel, out_shape=(jax.ShapeDtypeStruct((BLK, D), BF16), j...]
where the time goes in v5:
time: 49.2 us; the launch traced here: 49 us
  Pallas kernels  46 us (93%)
  local copies, waits for them, and re-layouts  2.37 us (5%)
  between operations  0.65 us (1%)
    pallas_call x1, Pallas kernels, body(): pl.pallas_call(kernel, out_shape=(jax.ShapeDtypeStruct((BLK, D), BF16), j...  46 us
    unnamed x4, local copies, waits for them, and re-layouts  2.37 us

profile of v5, /device:TPU:0, one launch (start us, length us, event | category | flops | bytes accessed | tf_op | source)
XLA Modules:
  0.0 49.0 jit_solution(9614107575486060853)
XLA Ops:
  0.6 46.0 %shard_map.86 = (bf16[96,2048]{1,0:T(8,128)(2,1)}, f32[4,384]{1,0:T(4,128)}) custom-call(bf16[96,2048]{1,0:T(8,128)(2,1)} %tok_hbm.1, bf16[2048,256]{1,0:T(8,128)(2,1)} %wq_hbm.1, bf16[64,2048]{1,0:T(8,128)(2,1)} %bitcast.2, bf16[64,2048]{1,0:T(8,128)(2,1)} %bitcast.3, bf16[256,2048]{1,0:T(8,128)(2,1)} %wo_hbm.1, bf16[4,64]{1,0:T(4,128)(2,1)} %qg_ref.1, ...), custom_call_target="tpu_custom_call" | custom-call | tf_op jit(solution)/shard_map/pallas_call | solution.py:393
  46.7 0.0 copy-start
  46.7 1.8 %copy.11 = bf16[96,2048]{1,0:T(8,128)(2,1)} copy(bf16[96,2048]{1,0:T(8,128)(2,1)} %get-tuple-element.4) | data formatting | bytes 786432
  48.4 0.0 copy-done
  48.4 0.6 %copy.12 = f32[4,384]{1,0:T(4,128)} copy(f32[4,384]{1,0:T(4,128)S(1)} %copy-done) | data formatting | bytes 12288
Async XLA Ops:
  46.7 1.8 %copy-start = (f32[4,384]{1,0:T(4,128)S(1)}, f32[4,384]{1,0:T(4,128)}, u32[]{:S(2)}) copy-start(f32[4,384]{1,0:T(4,128)} %get-tuple-element.5) | copy-start | bytes 18436

commit v6 on v5

--- a/solution.py
+++ b/solution.py
@@ -260,14 +260,19 @@
     sib0 = share(0)
     scores(0, slice(0, QT))
     tiles(0, 1)
+
+    def first_shared():
+        arrive(sib0)
+        tiles(1, 3)
+
+    pl.when(c == 0)(first_shared)
     arrive(one1)
     two1 = phase2(1)
     arrive([tok_r[1], tok_l[0]])
     project_keys(2)
     one2 = phase1(2)
     project_queries(2)
-    arrive(sib0)
-    tiles(1, 3)
+    pl.when(c == 1)(first_shared)
     arrive([tok_fr, tok_fl])
     copies[4].wait()
     wo_half = OUT_ROWS // 4
@@ -305,10 +310,10 @@
     tiles(17, 19)
     arrive(sib2)
     tiles(19, 23)
+    tiles(23, 25)
     arrive([wo_r[1], wo_l[0]])
     whole = pl.ds(pl.multiple_of(base, OUT_ROWS // 2), OUT_ROWS // 2)
     wsib = [send(wo.at[k, whole], wo.at[k, whole], wsib_sem.at[k - 1], sibling) for k in (1, 2)]
-    tiles(23, 25)
     arrive(sib3)
     tiles(25, 28)
     finish(2)

time: 49.2 us -> 48.8 us (level)
  Pallas kernels: 46 us -> 45.4 us
    pallas_call x1, Pallas kernels: 46 us -> 45.4 us  [body(): pl.pallas_call(kernel, out_shape=(jax.ShapeDtypeStruct((BLK, D), BF16), j...]
where the time goes in v6:
time: 48.8 us; the launch traced here: 48.4 us
  Pallas kernels  45.4 us (93%)
  local copies, waits for them, and re-layouts  2.37 us (5%)
  between operations  0.65 us (1%)
    pallas_call x1, Pallas kernels, body(): pl.pallas_call(kernel, out_shape=(jax.ShapeDtypeStruct((BLK, D), BF16), j...  45.4 us
    unnamed x4, local copies, waits for them, and re-layouts  2.37 us

profile of v6, /device:TPU:0, one launch (start us, length us, event | category | flops | bytes accessed | tf_op | source)
XLA Modules:
  0.0 48.4 jit_solution(18174209019637400040)
XLA Ops:
  0.6 45.4 %shard_map.86 = (bf16[96,2048]{1,0:T(8,128)(2,1)}, f32[4,384]{1,0:T(4,128)}) custom-call(bf16[96,2048]{1,0:T(8,128)(2,1)} %tok_hbm.1, bf16[2048,256]{1,0:T(8,128)(2,1)} %wq_hbm.1, bf16[64,2048]{1,0:T(8,128)(2,1)} %bitcast.2, bf16[64,2048]{1,0:T(8,128)(2,1)} %bitcast.3, bf16[256,2048]{1,0:T(8,128)(2,1)} %wo_hbm.1, bf16[4,64]{1,0:T(4,128)(2,1)} %qg_ref.1, ...), custom_call_target="tpu_custom_call" | custom-call | tf_op jit(solution)/shard_map/pallas_call | solution.py:398
  46.0 0.0 copy-start
  46.0 1.8 %copy.11 = bf16[96,2048]{1,0:T(8,128)(2,1)} copy(bf16[96,2048]{1,0:T(8,128)(2,1)} %get-tuple-element.4) | data formatting | bytes 786432
  47.8 0.0 copy-done
  47.8 0.6 %copy.12 = f32[4,384]{1,0:T(4,128)} copy(f32[4,384]{1,0:T(4,128)S(1)} %copy-done) | data formatting | bytes 12288
Async XLA Ops:
  46.0 1.8 %copy-start = (f32[4,384]{1,0:T(4,128)S(1)}, f32[4,384]{1,0:T(4,128)}, u32[]{:S(2)}) copy-start(f32[4,384]{1,0:T(4,128)} %get-tuple-element.5) | copy-start | bytes 18436
